TPU v7x, 512 devices: a whole 4x4x16 slice. The times are simulated.
512 devices in a mesh: sp: 32 (over z, core), tp: 16 (over y, x).
Axes of the slice: x: 4, y: 4, z: 16, core: 2. Of those that a mesh axis runs over, the one named last changes fastest.
Arguments:
- moe_input: bfloat16 [6144, 2048], P('sp'), may hold values from -6 to 6
- out_grad: bfloat16 [6144, 2048], P('sp'), may hold values from -6 to 6
- route_ids: int32 [6144, 2], P('sp'), may hold values from 0 to 31, all different within a row; in each aligned block of 192 rows (0 to 191, 192 to 383, ...) at most 18 rows name the same one
- route_weights: float32 [6144, 2], P('sp'), may hold values from 0.2 to 2
- expert_gate: bfloat16 [32, 2048, 2048], P('sp', None, 'tp'), may hold values from -0.125 to 0.125
- expert_up: bfloat16 [32, 2048, 2048], P('sp', None, 'tp'), may hold values from -0.125 to 0.125
- expert_down: bfloat16 [32, 2048, 2048], P('sp', 'tp'), may hold values from -0.125 to 0.125
- proj_weight: bfloat16 [1024, 2048], P(None, 'tp'), may hold values from -0.1875 to 0.1875
- glu_value: bfloat16 [1024, 6144], P('tp', 'sp'), may hold values from -6 to 6
- glu_gate: bfloat16 [1024, 6144], P('tp', 'sp'), may hold values from -8 to 8
- conv_taps: float32 [1024, 31], P('tp'), may hold values from -1 to 1
- norm_input: bfloat16 [1024, 6144], P('tp', 'sp'), may hold values from -6 to 6
- norm_gain: float32 [1024], replicated, may hold values from 0.1 to 1.9
Outputs:
- grad_gate: bfloat16 [32, 2048, 2048], P('sp', None, 'tp')
- grad_up: bfloat16 [32, 2048, 2048], P('sp', None, 'tp')
- grad_down: bfloat16 [32, 2048, 2048], P('sp', 'tp')
- grad_proj: float32 [1024, 2048], P('sp', 'tp')
- grad_value: bfloat16 [1024, 6144], P('tp', 'sp')
- grad_glu_gate: bfloat16 [1024, 6144], P('tp', 'sp')
Inputs may be any that keep to these rules, and one draw needn't show every extreme that they name: `route_ids`: within the rows of one device, the 2 ids of a position differ and no expert is named by more than 18 pairs; some expert is named by exactly 18.
All inputs are finite; a program needn't handle non-finite values.
Results may differ from a plain program's by a relative error of at most 0.025.
Values may be sent and summed in bfloat16 or wider, within the bound.
No kernel may reach another device: no remote copies, remote signals or barrier semaphores. Data moves between devices by JAX's collectives and lax.ppermute only.
A program may use at most 64 MiB of HBM per device.

v0:
```python
import jax
import jax.numpy as jnp
from jax import lax
from jax.experimental import pallas as pl
from jax.experimental.pallas import tpu as pltpu
from jax.sharding import Mesh
from jax.sharding import PartitionSpec as P

TP = ("ty", "tx")
SP = ("z", "core")
PLANE = ("core", "ty", "tx")


norm_eps = 1e-05

bf16, f32, i32 = jnp.bfloat16, jnp.float32, jnp.int32


def exchanged(blocks, axis, index_groups=None):
    return lax.all_to_all(blocks, axis, 0, 0, axis_index_groups=index_groups, tiled=True)


def line_groups(ny, nx):
    along_x = [[y * nx + x for x in range(nx)] for y in range(ny)]
    along_y = [[y * nx + x for y in range(ny)] for x in range(nx)]

    def of_core_one(lines):
        return [[ny * nx + i for i in line] for line in lines]

    return along_x + of_core_one(along_y), along_y + of_core_one(along_x)


def line_pairs(ny, nx, by):
    pairs = []
    for y in range(ny):
        for x in range(nx):
            pairs.append((y * nx + x, y * nx + (x + by) % nx))
            pairs.append((ny * nx + y * nx + x, ny * nx + (y + by) % ny * nx + x))
    return pairs


def silu_grad(pre):
    sig = jax.nn.sigmoid(pre)
    return sig * (1.0 + pre * (1.0 - sig))


def contract(a, b, dim_a, dim_b):
    return lax.dot_general(a, b, (((dim_a,), (dim_b,)), ((), ())), preferred_element_type=f32)


def iota(shape, dim):
    return lax.broadcasted_iota(i32, shape, dim)


def whole():
    return pl.BlockSpec(memory_space=pltpu.VMEM)


def scalar():
    return pl.BlockSpec(memory_space=pltpu.SMEM)


def params(mib):
    return pltpu.CompilerParams(vmem_limit_bytes=mib * 1024 * 1024)


def cost(flops, size):
    return pl.CostEstimate(flops=flops, bytes_accessed=size, transcendentals=0)


def one_if(condition):
    return jnp.where(condition, 1.0, 0.0).astype(bf16)


def prep_kernel(lane_ref, ids_hbm, scale_hbm, input_hbm, grad_hbm, *refs, experts):
    sent_ref, back_ref, own_ref, ids_ref, scale_ref, input_ref, sems = refs
    tok, width = input_ref.shape
    columns = pl.ds(pl.multiple_of(lane_ref[0] * width, width), width)
    copies = [
        pltpu.make_async_copy(ids_hbm, ids_ref, sems.at[0]),
        pltpu.make_async_copy(scale_hbm, scale_ref, sems.at[1]),
        pltpu.make_async_copy(input_hbm.at[:, columns], input_ref, sems.at[2]),
        pltpu.make_async_copy(grad_hbm.at[:, columns], own_ref, sems.at[3]),
    ]
    for copy in copies:
        copy.start()
    for copy in copies:
        copy.wait()
    e0, e1 = ids_ref[0:1, :], ids_ref[1:2, :]
    s0, s1 = scale_ref[0:1, :], scale_ref[1:2, :]
    rows = iota((experts, tok), 0)
    hit0, hit1 = rows == e0, rows == e1
    earlier = one_if(iota((tok, tok), 0) < iota((tok, tok), 1))
    before = jnp.dot(one_if(hit0 | hit1), earlier, preferred_element_type=f32)
    slot0 = jnp.sum(jnp.where(hit0, before, 0.0), axis=0, keepdims=True).astype(i32)
    slot1 = jnp.sum(jnp.where(hit1, before, 0.0), axis=0, keepdims=True).astype(i32)
    x = input_ref[...]
    grad = own_ref[...]
    diagonal = iota((tok, tok), 0) == iota((tok, tok), 1)
    c0 = jnp.sum(jnp.where(diagonal, s0, 0.0), axis=1, keepdims=True)
    c1 = jnp.sum(jnp.where(diagonal, s1, 0.0), axis=1, keepdims=True)
    g = grad.astype(f32)
    g0, g1 = (g * c0).astype(bf16), (g * c1).astype(bf16)
    pitch = sent_ref.shape[0] // experts
    r = iota((sent_ref.shape[0], tok), 0)
    a0, a1 = e0 * pitch + slot0, e1 * pitch + slot1
    half = pitch // 2
    sent = jnp.dot(one_if((r == a0) | (r == a1)), x, preferred_element_type=f32)
    sent = sent + jnp.dot(one_if(r == a0 + half), g0, preferred_element_type=f32)
    sent = sent + jnp.dot(one_if(r == a1 + half), g1, preferred_element_type=f32)
    sent_ref[...] = sent.astype(bf16)
    back_pitch = back_ref.shape[0] // experts
    r = iota((back_ref.shape[0], tok), 0)
    back_ref[...] = one_if((r == e0 * back_pitch + slot0) | (r == e1 * back_pitch + slot1))


def packed(block):
    lanes = 128
    wide = block[:, :lanes]
    rest = block[:, lanes:]
    rows = rest.shape[0] // 2
    return wide, jnp.concatenate([rest[:rows], rest[rows:]], axis=1)


def unpacked(wide, rest):
    lanes = rest.shape[1] // 2
    tail = jnp.concatenate([rest[:, :lanes], rest[:, lanes:]], axis=0)
    return jnp.concatenate([wide, tail], axis=1)


def compact_kernel(part_ref, norm_ref, out_ref, *, capacity, pitch):
    count = out_ref.shape[0]
    rows_in = part_ref.shape[0] // count
    rows_out = rows_in // pitch * capacity
    into, outof = iota((rows_out, rows_in), 0), iota((rows_out, rows_in), 1)
    pick_x = one_if(outof == (into // capacity) * pitch + into % capacity)
    pick_g = one_if(outof == (into // capacity) * pitch + into % capacity + pitch // 2)
    wide, rest = packed(norm_ref[...].astype(f32))
    wide, rest = wide.astype(bf16), rest.astype(bf16)
    for q in range(count):
        piece = part_ref[pl.ds(q * rows_in, rows_in), :]
        out_ref[q, pl.ds(0, rows_out), :] = jnp.dot(pick_x, piece, preferred_element_type=f32).astype(bf16)
        out_ref[q, pl.ds(rows_out, rows_out), :] = jnp.dot(pick_g, piece, preferred_element_type=f32).astype(bf16)
        out_ref[q, pl.ds(2 * rows_out, wide.shape[0]), :] = wide
        out_ref[q, pl.ds(2 * rows_out + wide.shape[0], rest.shape[0]), :] = rest


def pieces_of(core_ref, ny, nx):
    core = core_ref[0]
    return [
        (jnp.where(core == 0, y, x), jnp.where(core == 0, x, y)) for y in range(ny) for x in range(nx)
    ]


def pack_kernel(gate_ref, up_ref, down_ref, out_ref):
    height, width = gate_ref.shape
    out_ref[pl.ds(0, height), :] = gate_ref[...]
    out_ref[pl.ds(height, height), :] = up_ref[...]
    for k in range(height // width):
        out_ref[pl.ds(2 * height + k * width, width), :] = down_ref[:, pl.ds(k * width, width)]


def expert_kernel(core_ref, rows_ref, *refs):
    weights_hbm = refs[0:5]
    back_ref, hidden_ref, both_ref = refs[5:8]
    weights, acc_ref, sems = refs[8:12], refs[12], refs[13]
    middle = weights_hbm[3].shape[0]
    targets = (*weights[:3], weights[3].at[pl.ds(0, middle)], weights[3].at[pl.ds(middle, middle)])
    copies = [
        pltpu.make_async_copy(source, target, sems.at[i])
        for i, (source, target) in enumerate(zip(weights_hbm, targets, strict=True))
    ]
    for copy in copies:
        copy.start()
    ny, nx, _, width = rows_ref.shape
    count = hidden_ref.shape[0]
    pieces = pieces_of(core_ref, ny, nx)
    height = ny * nx * width
    x = jnp.concatenate([rows_ref[a, b, pl.ds(0, count), :] for a, b in pieces], axis=1)
    g = jnp.concatenate([rows_ref[a, b, pl.ds(count, count), :] for a, b in pieces], axis=1)
    for k, block in enumerate(weights):
        copies[k].wait()
        if k == 3:
            copies[4].wait()
        w_both = jnp.concatenate([block[pl.ds(0, height), :], block[pl.ds(height, height), :]], axis=1)
        w_down = jnp.concatenate(
            [block[pl.ds(2 * height + i * width, width), :] for i in range(ny * nx)], axis=1
        )
        pre = jnp.dot(x, w_both, preferred_element_type=f32)
        gate_pre, up_pre = pre[:, :width], pre[:, width:]
        d_hidden = contract(g, w_down, 1, 1)
        sig = jax.nn.sigmoid(gate_pre)
        gate_act = gate_pre * sig
        hidden_ref[:, pl.ds(k * width, width)] = (gate_act * up_pre).astype(bf16)
        d_gate = d_hidden * up_pre * (sig * (1.0 + gate_pre * (1.0 - sig)))
        d_up = d_hidden * gate_act
        both = jnp.concatenate([d_gate.astype(bf16), d_up.astype(bf16)], axis=1)
        both_ref[:, pl.ds(2 * k * width, 2 * width)] = both
        back = contract(both, w_both, 1, 1)
        acc_ref[...] = back if k == 0 else acc_ref[...] + back
    for j, (a, b) in enumerate(pieces):
        back_ref[a, b] = acc_ref[:, pl.ds(j * width, width)].astype(bf16)


def row_pack_kernel(core_ref, rows_ref, hidden_ref, both_ref, onward_ref, backward_ref, across_ref):
    ny, nx, _, width = rows_ref.shape
    count = hidden_ref.shape[0]
    for j, (a, b) in enumerate(pieces_of(core_ref, ny, nx)):
        rows = rows_ref[a, b, pl.ds(0, 2 * count), :]
        onward_ref[pl.ds(2 * j * count, 2 * count), :] = rows
        backward_ref[pl.ds(2 * j * count, 2 * count), :] = rows
    start = 2 * ny * nx * count
    for k, out_ref, at in ((2, onward_ref, start), (1, backward_ref, start), (3, across_ref, 0)):
        out_ref[pl.ds(at, count), :] = hidden_ref[:, pl.ds(k * width, width)]
        out_ref[pl.ds(at + count, count), :] = both_ref[:, pl.ds(2 * k * width, width)]
        out_ref[pl.ds(at + 2 * count, count), :] = both_ref[:, pl.ds((2 * k + 1) * width, width)]


def weight_kernel(own_ref, behind_ref, ahead_ref, low_ref, high_ref, across_ref, hidden_ref, both_ref, *outs):
    gate_ref, up_ref, down_ref = outs
    count, width = hidden_ref.shape[0], own_ref.shape[1]
    number = down_ref.shape[1] // width
    start = 2 * number * count

    def units(part, own):
        at = part * count
        return jnp.concatenate(
            [
                own,
                behind_ref[pl.ds(start + at, count), :],
                ahead_ref[pl.ds(start + at, count), :],
                across_ref[pl.ds(at, count), :],
            ],
            axis=0,
        )

    hidden = units(0, hidden_ref[:, :width])
    both = jnp.concatenate(
        [units(1, both_ref[:, :width]), units(2, both_ref[:, width : 2 * width])], axis=1
    )
    half = number // 2
    for j in range(number):
        far_ref, i = (low_ref, j) if j < half else (high_ref, j - half)

        def rows(part):
            at = (2 * j + part) * count
            near = [ref[pl.ds(at, count), :] for ref in (own_ref, behind_ref, ahead_ref)]
            return jnp.concatenate([*near, far_ref[pl.ds((2 * i + part) * count, count), :]], axis=0)

        pair = contract(rows(0), both, 0, 0)
        at = pl.ds(j * width, width)
        gate_ref[at, :] = pair[:, :width].astype(bf16)
        up_ref[at, :] = pair[:, width:].astype(bf16)
        down_ref[:, at] = contract(hidden, rows(1), 0, 0).astype(bf16)


def norm_kernel(core_ref, parts_ref, gain_ref, act_ref, slope_ref, cross_ref, stats_ref):
    ny, nx, height, _ = parts_ref.shape
    part = height * 2 // 3
    blocks = []
    for a, b in pieces_of(core_ref, ny, nx):
        block = parts_ref[a, b].astype(f32)
        blocks.append(unpacked(block[:part], block[part:]))
    values = jnp.concatenate(blocks, axis=0)
    channels = values.shape[0]
    mean = jnp.sum(values, axis=0, keepdims=True) / channels
    centred = values - mean
    inv = lax.rsqrt(jnp.sum(centred * centred, axis=0, keepdims=True) / channels + norm_eps)
    gain = gain_ref[...]
    normed = centred * inv
    scaled = normed * gain
    sig = jax.nn.sigmoid(scaled)
    act_ref[...] = (scaled * sig).astype(bf16)
    slope = sig * (1.0 + scaled * (1.0 - sig)) * gain
    slope_ref[...] = slope.astype(bf16)
    cross_ref[...] = (slope * normed).astype(bf16)
    stats_ref[0:1, :] = mean
    stats_ref[1:2, :] = inv


def line_sum_kernel(parts_ref, out_ref):
    acc = parts_ref[0].astype(f32)
    for j in range(1, parts_ref.shape[0]):
        acc = acc + parts_ref[j].astype(f32)
    out_ref[...] = acc.astype(bf16)


def spread_kernel(rows_ref, out_ref, *, capacity, pitch):
    count, rows_in, _ = rows_ref.shape
    rows_out = rows_in // capacity * pitch
    into, outof = iota((rows_out, rows_in), 0), iota((rows_out, rows_in), 1)
    spread = one_if((outof == (into // pitch) * capacity + into % pitch) & (into % pitch < capacity))
    for q in range(count):
        moved = jnp.dot(spread, rows_ref[q], preferred_element_type=f32)
        out_ref[pl.ds(q * rows_out, rows_out), :] = moved.astype(bf16)


def mix_kernel(core_ref, *refs):
    sources, outs, local, sems = refs[:7], refs[7:10], refs[10:17], refs[17]
    kept_ref, given_ref, blocks_ref = outs
    back_ref, returned_ref, own_ref, proj_ref, slope_ref, cross_ref, act_ref = local
    core = core_ref[0]
    copies = [
        pltpu.make_async_copy(source, target, sems.at[i])
        for i, (source, target) in enumerate(zip(sources, local, strict=True))
    ]
    for copy in copies:
        copy.start()
    for copy in copies[:3]:
        copy.wait()
    moe = contract(back_ref[...], returned_ref[...], 0, 0)
    mix = (own_ref[...].astype(f32) + moe).astype(bf16)
    for copy in copies[3:]:
        copy.wait()
    d_act = contract(proj_ref[...], mix, 1, 1)
    lanes = 128

    def as_rows(line):
        rest = line[:, lanes:]
        return [line[:, :lanes], jnp.concatenate([rest, jnp.zeros_like(rest)], axis=1)]

    tail = []
    for ref in (slope_ref, cross_ref):
        line = jnp.sum(ref[...].astype(f32) * d_act, axis=0, keepdims=True)
        high = line.astype(bf16).astype(f32)
        tail += as_rows(high) + as_rows(line - high)
    tail = jnp.concatenate(tail, axis=0).astype(bf16)
    count = blocks_ref.shape[0]
    part = d_act.shape[0] // count
    for j in range(count):
        wide, rest = packed(d_act[j * part : (j + 1) * part])
        blocks_ref[j, pl.ds(0, part), :] = wide.astype(bf16)
        blocks_ref[j, pl.ds(part, part // 2), :] = rest.astype(bf16)
        blocks_ref[j, pl.ds(part * 3 // 2, 8), :] = tail
    grad = jnp.dot(act_ref[...], mix, preferred_element_type=f32)
    size = kept_ref.shape[1]
    for k in range(kept_ref.shape[0]):
        even = grad[2 * k * size : (2 * k + 1) * size]
        odd = grad[(2 * k + 1) * size : (2 * k + 2) * size]
        kept_ref[k] = jnp.where(core == 0, even, odd).astype(bf16)
        given_ref[k] = jnp.where(core == 0, odd, even).astype(bf16)


def conv_grad_kernel(blocks_ref, norm_ref, gain_ref, stats_ref, out_ref, head_ref, *, channels):
    count, _, _ = blocks_ref.shape
    acc = blocks_ref[0].astype(f32)
    for j in range(1, count):
        acc = acc + blocks_ref[j].astype(f32)
    part = out_ref.shape[0]
    grad_act = unpacked(acc[:part], acc[part : part * 3 // 2])
    tail = acc[part * 3 // 2 :]

    def line(at):
        rest = tail[at + 1 : at + 2] + tail[at + 3 : at + 4]
        return jnp.concatenate([tail[at : at + 1] + tail[at + 2 : at + 3], rest[:, : rest.shape[1] // 2]], axis=1)

    mean, inv = stats_ref[0:1, :], stats_ref[1:2, :]
    gain = gain_ref[...]
    normed = (norm_ref[...].astype(f32) - mean) * inv
    grad_normed = grad_act * silu_grad(normed * gain) * gain
    out = inv * (grad_normed - line(0) / channels - normed * (line(4) / channels))
    out_ref[...] = out
    head_ref[...] = out[:, : head_ref.shape[1]]


def body(
    moe_input,
    out_grad,
    route_ids,
    route_weights,
    expert_gate,
    expert_up,
    expert_down,
    proj_weight,
    glu_value,
    glu_gate,
    conv_taps,
    norm_input,
    norm_gain,
):
    groups = lax.axis_size(SP)
    ny, nx = lax.axis_size("ty"), lax.axis_size("tx")
    lane_count = ny * nx
    lane_index = lax.axis_index(TP)
    tok_rows, model_width = moe_input.shape
    top_count = route_ids.shape[1]
    capacity = tok_rows * top_count * 3 // (2 * groups)
    total = groups * capacity
    width = model_width // lane_count
    pitch = 40
    back_pitch = 24
    channel_part = norm_input.shape[0]
    channels = channel_part * lane_count
    struct = jax.ShapeDtypeStruct

    sent, back_place, own_grad = pl.pallas_call(
        lambda *refs: prep_kernel(*refs, experts=groups),
        in_specs=[scalar()] + [pl.BlockSpec(memory_space=pltpu.HBM)] * 4,
        out_specs=[whole()] * 3,
        out_shape=[
            struct((groups * pitch, width), bf16),
            struct((groups * back_pitch, tok_rows), bf16),
            struct((tok_rows, width), bf16),
        ],
        scratch_shapes=[
            pltpu.VMEM((top_count, tok_rows), i32),
            pltpu.VMEM((top_count, tok_rows), f32),
            pltpu.VMEM((tok_rows, width), bf16),
            pltpu.SemaphoreType.DMA((4,)),
        ],
        compiler_params=params(58),
        name="prep",
    )(lane_index.astype(i32).reshape(1), route_ids.T, route_weights.T, moe_input, out_grad)

    part = exchanged(sent.reshape(groups, pitch, width), SP)

    core = lax.axis_index("core").astype(i32).reshape(1)
    first_groups, second_groups = line_groups(ny, nx)
    w_gate, w_up, w_down = expert_gate[0], expert_up[0], expert_down[0]
    ff = w_gate.shape[1]
    hbm = pl.BlockSpec(memory_space=pltpu.HBM)
    w_gate, w_up, w_down, _ = lax.optimization_barrier((w_gate, w_up, w_down, sent))
    own_weights = pl.pallas_call(
        pack_kernel,
        out_shape=struct((3 * model_width, ff), bf16),
        in_specs=[whole()] * 3,
        out_specs=whole(),
        compiler_params=params(58),
        cost_estimate=cost(8 * total * model_width * ff, 6 * model_width * ff),
        name="pack",
    )(w_gate, w_up, w_down)
    onward, backward, across = [line_pairs(ny, nx, by) for by in (1, -1, 2)]
    weights = (
        own_weights,
        lax.ppermute(own_weights, PLANE, onward),
        lax.ppermute(own_weights, PLANE, backward),
    )

    quarter = total // nx
    norm_rows = channel_part * 3 // 2
    rows_height = 2 * quarter + norm_rows
    quarters = pl.pallas_call(
        lambda *refs: compact_kernel(*refs, capacity=capacity, pitch=pitch),
        out_shape=struct((nx, rows_height, width), bf16),
        in_specs=[whole(), whole()],
        out_specs=whole(),
        compiler_params=params(16),
        name="compact",
    )(part.reshape(groups * pitch, width), norm_input)
    quarters, *weights = lax.optimization_barrier((exchanged(quarters, PLANE, first_groups), *weights))
    middle = weights[0].shape[0] // 2
    weights += [
        lax.ppermute(weights[1][:middle], PLANE, onward),
        lax.ppermute(weights[2][middle:], PLANE, backward),
    ]
    gathered = exchanged(jnp.broadcast_to(quarters[None], (ny, *quarters.shape)), PLANE, second_groups)

    packed_weights = pltpu.VMEM((3 * model_width, ff), bf16)
    back, hidden, both = pl.pallas_call(
        expert_kernel,
        in_specs=[scalar(), whole()] + [hbm] * 5,
        out_specs=[whole()] * 3,
        out_shape=[
            struct((ny, nx, quarter, width), bf16),
            struct((quarter, nx * ff), bf16),
            struct((quarter, 2 * nx * ff), bf16),
        ],
        scratch_shapes=[
            packed_weights,
            packed_weights,
            packed_weights,
            packed_weights,
            pltpu.VMEM((quarter, model_width), f32),
            pltpu.SemaphoreType.DMA((5,)),
        ],
        compiler_params=params(50),
        cost_estimate=cost(10 * total * model_width * ff, 10 * total * model_width),
        name="expert",
    )(core, gathered, *weights)

    line_parts = exchanged(back, PLANE, second_groups)
    unit_rows = 3 * quarter
    buffer_rows = 2 * lane_count * quarter + unit_rows
    to_onward, to_backward, to_across = pl.pallas_call(
        row_pack_kernel,
        in_specs=[scalar()] + [whole()] * 3,
        out_specs=[whole()] * 3,
        out_shape=[
            struct((buffer_rows, width), bf16),
            struct((buffer_rows, width), bf16),
            struct((unit_rows, width), bf16),
        ],
        compiler_params=params(58),
        cost_estimate=cost(6 * total * model_width * ff, 10 * total * model_width),
        name="row_pack",
    )(core, gathered, hidden, both)
    line_parts, to_onward, to_backward, to_across = lax.optimization_barrier(
        (line_parts, to_onward, to_backward, to_across)
    )
    line_rows = pl.pallas_call(
        line_sum_kernel,
        out_shape=struct((nx, quarter, width), bf16),
        in_specs=[whole()],
        out_specs=whole(),
        compiler_params=params(16),
        name="line_sum",
    )(line_parts)
    own_rows = exchanged(line_rows, PLANE, first_groups)
    summed_grad = pl.pallas_call(
        lambda *refs: spread_kernel(*refs, capacity=capacity, pitch=back_pitch),
        out_shape=struct((groups * back_pitch, width), bf16),
        in_specs=[whole()],
        out_specs=whole(),
        compiler_params=params(16),
        name="spread",
    )(own_rows)
    returned = exchanged(summed_grad.reshape(groups, back_pitch, width), SP)

    own_buffer = to_onward
    summed_grad, to_onward, to_backward, to_across = lax.optimization_barrier(
        (summed_grad, to_onward, to_backward, to_across)
    )
    from_behind = lax.ppermute(to_onward, PLANE, onward)
    from_ahead = lax.ppermute(to_backward, PLANE, backward)
    from_across = lax.ppermute(to_across, PLANE, across)
    far_rows = lane_count * quarter
    far_low = lax.ppermute(from_behind[:far_rows], PLANE, onward)
    far_high = lax.ppermute(from_ahead[far_rows : 2 * far_rows], PLANE, backward)

    act, slope, cross, stats = pl.pallas_call(
        norm_kernel,
        grid_spec=pltpu.PrefetchScalarGridSpec(
            num_scalar_prefetch=1,
            grid=(1,),
            in_specs=[
                pl.BlockSpec((ny, nx, norm_rows, width), lambda i, m: (0, 0, 2 * quarter // norm_rows, 0)),
                pl.BlockSpec((channels, 1), lambda i, m: (0, 0)),
            ],
            out_specs=[pl.BlockSpec((channels, tok_rows), lambda i, m: (0, 0))] * 3
            + [pl.BlockSpec((2, tok_rows), lambda i, m: (0, 0))],
        ),
        out_shape=[struct((channels, tok_rows), bf16)] * 3 + [struct((2, tok_rows), f32)],
        compiler_params=params(58),
        cost_estimate=cost(6 * total * model_width * ff, 10 * total * model_width),
        name="norm",
    )(core, gathered, norm_gain[:, None])

    proj_size = channels // groups
    block_rows = norm_rows + 8
    mix_inputs = (
        back_place,
        returned.reshape(groups * back_pitch, width),
        own_grad,
        proj_weight,
        slope,
        cross,
        act,
    )
    kept, given, blocks = pl.pallas_call(
        mix_kernel,
        out_shape=[
            struct((groups // 2, proj_size, width), bf16),
            struct((groups // 2, proj_size, width), bf16),
            struct((lane_count, block_rows, width), bf16),
        ],
        in_specs=[scalar()] + [pl.BlockSpec(memory_space=pltpu.HBM)] * len(mix_inputs),
        out_specs=[whole()] * 3,
        scratch_shapes=[pltpu.VMEM(value.shape, value.dtype) for value in mix_inputs]
        + [pltpu.SemaphoreType.DMA((len(mix_inputs),))],
        compiler_params=params(58),
        name="mix",
    )(core, *mix_inputs)
    arrived = exchanged(blocks, TP)
    from_pair = lax.ppermute(given, "core", [(0, 1), (1, 0)])
    chip_sum = (kept.astype(f32) + from_pair.astype(f32)).astype(bf16)
    chip_sum, arrived = lax.optimization_barrier((chip_sum, arrived))
    proj_parts = exchanged(chip_sum, "z")
    grad_proj = jnp.sum(proj_parts.astype(f32), axis=0)

    taps_count = conv_taps.shape[1]
    reach_back = taps_count - 1
    gain_own = lax.dynamic_slice_in_dim(norm_gain, lane_index * channel_part, channel_part, 0)
    grad_conv, head = pl.pallas_call(
        lambda *refs: conv_grad_kernel(*refs, channels=channels),
        out_shape=[struct((channel_part, tok_rows), f32), struct((channel_part, reach_back), f32)],
        in_specs=[whole()] * 4,
        out_specs=[whole()] * 2,
        compiler_params=params(16),
        name="conv_grad",
    )(arrived, norm_input, gain_own[:, None], stats)

    pairs = [(i, i - 1) for i in range(1, groups)]
    ahead_rows = lax.ppermute(head, SP, pairs)
    extended = jnp.concatenate([grad_conv, ahead_rows], axis=1)
    grad_glu = jnp.zeros_like(grad_conv)
    for tap_index in range(taps_count):
        grad_glu = (
            grad_glu
            + conv_taps[:, tap_index : tap_index + 1]
            * extended[:, reach_back - tap_index : reach_back - tap_index + tok_rows]
        )
    sigmoid_gate = jax.nn.sigmoid(glu_gate.astype(f32))
    grad_value = (grad_glu * sigmoid_gate).astype(bf16)
    grad_glu_gate = (
        grad_glu * glu_value.astype(f32) * sigmoid_gate * (1.0 - sigmoid_gate)
    ).astype(bf16)
    gate_wgrad, up_wgrad, down_grad = pl.pallas_call(
        weight_kernel,
        in_specs=[whole()] * 8,
        out_specs=[whole()] * 3,
        out_shape=[
            struct((model_width, ff), bf16),
            struct((model_width, ff), bf16),
            struct((ff, model_width), bf16),
        ],
        compiler_params=params(58),
        cost_estimate=cost(6 * total * model_width * ff, 10 * total * model_width),
        name="weight_sum",
    )(own_buffer, from_behind, from_ahead, far_low, far_high, from_across, hidden, both)
    return (gate_wgrad[None], up_wgrad[None], down_grad[None], grad_proj, grad_value, grad_glu_gate)


def solution(mesh):
    finer = Mesh(mesh.devices.reshape(mesh.shape["sp"] // 2, 2, 4, 4), ("z", "core", "ty", "tx"))
    return jax.shard_map(
        body,
        mesh=finer,
        in_specs=(
            P(SP, None),
            P(SP, None),
            P(SP, None),
            P(SP, None),
            P(SP, None, TP),
            P(SP, None, TP),
            P(SP, TP, None),
            P(None, TP),
            P(TP, SP),
            P(TP, SP),
            P(TP, None),
            P(TP, SP),
            P(),
        ),
        out_specs=(
            P(SP, None, TP),
            P(SP, None, TP),
            P(SP, TP, None),
            P(SP, TP),
            P(TP, SP),
            P(TP, SP),
        ),
        check_vma=False,
    )
```

profile of v0, /device:TPU:1, one launch (start us, length us, event | category | flops | bytes accessed | tf_op | source)
XLA Modules:
  0.0 204.9 jit_solution(7042710205694725040)
XLA Ops:
  0.6 2.6 %prep.1 = (bf16[1280,128]{1,0:T(8,128)(2,1)}, bf16[768,192]{1,0:T(8,128)(2,1)}, bf16[192,128]{1,0:T(8,128)(2,1)}) custom-call(s32[1]{0:T(128)} %bitcast.1.refs_0_, s32[2,192]{1,0:T(2,128)} %bitcast.83, f32[2,192]{1,0:T(2,128)} %bitcast.84, bf16[192,2048]{1,0:T(8,128)(2,1)} %refs_3_.2, bf16[192,2048]{1,0:T(8,128)(2,1)} %refs_4_.1), custom_call_target="tpu_custom_call" | custom-call | tf_op jit(solution)/shard_map/prep/pallas_call | solution.py:396
  3.2 2.7 %pack.1.refs_0_ = bf16[6144,128]{1,0:T(8,128)(2,1)} custom-call(bf16[2048,128]{1,0:T(8,128)(2,1)} %bitcast.85, bf16[2048,128]{1,0:T(8,128)(2,1)} %bitcast.86, bf16[128,2048]{1,0:T(8,128)(2,1)} %bitcast.87), custom_call_target="tpu_custom_call" | custom-call | flops 1207959552 | bytes 1572864 | tf_op jit(solution)/shard_map/pack/pallas_call | solution.py:423
  5.9 4.0 %collective-permute-start = (bf16[6144,128]{1,0:T(8,128)(2,1)}, bf16[6144,128]{1,0:T(8,128)(2,1)S(1)}, u32[]{:S(2)}, u32[]{:S(2)}) collective-permute-start(bf16[6144,128]{1,0:T(8,128)(2,1)} %pack.1.refs_0_), channel_id=1, source_target_pairs={{0,1},{16,20},{1,2},{17,21},{2,3},{18,22},{3,0},{19,23},{4,5},{20,... | collective-permute-start | bytes 4718600 | tf_op jit(solution)/shard_map/ppermute | solution.py:435
  10.0 3.4 %collective-permute-start.1 = (bf16[6144,128]{1,0:T(8,128)(2,1)}, bf16[6144,128]{1,0:T(8,128)(2,1)}, u32[]{:S(2)}, u32[]{:S(2)}) collective-permute-start(bf16[6144,128]{1,0:T(8,128)(2,1)} %pack.1.refs_0_), channel_id=1, source_target_pairs={{0,3},{16,28},{1,0},{17,29},{2,1},{18,30},{3,2},{19,31},{4,7},{20,... | collective-permute-start | bytes 4718600 | tf_op jit(solution)/shard_map/ppermute | solution.py:436
  13.3 41.2 %all_to_all.40 = bf16[32,40,128]{2,1,0:T(8,128)(2,1)S(1)} all-to-all(bf16[32,40,128]{2,1,0:T(8,128)(2,1)S(1)} %bitcast.81), channel_id=1, replica_groups=mesh['z'=16,'core'=2,'ty'=4,'tx'=4] {'z','core'}, dimensions={0} | all-to-all | bytes 655360 | tf_op jit(solution)/shard_map/all_to_all | solution.py:20
  54.5 0.5 compact.1
  55.0 10.5 %all_to_all.41 = bf16[4,384,128]{2,1,0:T(8,128)(2,1)S(1)} all-to-all(bf16[4,384,128]{2,1,0:T(8,128)(2,1)S(1)} %compact.1), channel_id=1, replica_groups={{0,1,2,3},{4,5,6,7},{8,9,10,11},{12,13,14,15},{16,20,24,28},{17,21,25,2..., dimensions={0} | all-to-all | bytes 786432 | tf_op jit(solution)/shard_map/all_to_all | solution.py:20
  65.5 1.7 broadcast_in_dim.21
  67.2 3.6 %all-to-all-start.2 = ((bf16[4,4,384,128]{3,2,1,0:T(8,128)(2,1)}), bf16[4,4,384,128]{3,2,1,0:T(8,128)(2,1)S(1)}, u32[]{:S(2)}, u32[]{:S(2)}) async-start(bf16[4,4,384,128]{3,2,1,0:T(8,128)(2,1)} %broadcast_in_dim.21), calls=%async_computation.2 | async-start | bytes 3145728 | tf_op jit(solution)/shard_map/all_to_all | solution.py:20
  70.8 0.9 slice.195
  71.7 2.2 %collective-permute-start.2 = (bf16[3072,128]{1,0:T(8,128)(2,1)}, bf16[3072,128]{1,0:T(8,128)(2,1)S(1)}, u32[]{:S(2)}, u32[]{:S(2)}) collective-permute-start(bf16[3072,128]{1,0:T(8,128)(2,1)} %slice.195), channel_id=1, source_target_pairs={{0,1},{16,20},{1,2},{17,21},{2,3},{18,22},{3,0},{19,23},{4,5},{20,... | collective-permute-start | bytes 2359304 | tf_op jit(solution)/shard_map/ppermute | solution.py:453
  73.9 2.1 %slice.196 = bf16[3072,128]{1,0:T(8,128)(2,1)} slice(bf16[6144,128]{1,0:T(8,128)(2,1)} %collective-permute-done.1.refs_2_), slice={[3072:6144], [0:128]} | slice | bytes 1572864 | tf_op jit(solution)/shard_map/slice | solution.py:454
  76.0 4.3 %collective-permute-start.3 = (bf16[3072,128]{1,0:T(8,128)(2,1)}, bf16[3072,128]{1,0:T(8,128)(2,1)S(1)}, u32[]{:S(2)}, u32[]{:S(2)}) collective-permute-start(bf16[3072,128]{1,0:T(8,128)(2,1)} %slice.196), channel_id=1, source_target_pairs={{0,3},{16,28},{1,0},{17,29},{2,1},{18,30},{3,2},{19,31},{4,7},{20,... | collective-permute-start | bytes 2359304 | tf_op jit(solution)/shard_map/ppermute | solution.py:454
  80.3 13.0 %collective-permute-done.2.refs_3_ = bf16[3072,128]{1,0:T(8,128)(2,1)S(1)} collective-permute-done((bf16[3072,128]{1,0:T(8,128)(2,1)}, bf16[3072,128]{1,0:T(8,128)(2,1)S(1)}, u32[]{:S(2)}, u32[]{:S(2)}) %collective-permute-start.2) | collective-permute-done | bytes 786464 | tf_op jit(solution)/shard_map/ppermute | solution.py:453
  93.3 1.2 copy-done.4
  94.5 6.8 %expert.1 = (bf16[4,4,144,128]{3,2,1,0:T(8,128)(2,1)}, bf16[144,512]{1,0:T(8,128)(2,1)S(1)}, bf16[144,1024]{1,0:T(8,128)(2,1)S(1)}) custom-call(s32[1]{0:T(128)} %bitcast.core_ref, bf16[4,4,384,128]{3,2,1,0:T(8,128)(2,1)} %copy-done.4, bf16[6144,128]{1,0:T(8,128)(2,1)} %pack.1.refs_0_, bf16[6144,128]{1,0:T(8,128)(2,1)} %copy-done.5, ...), custom_call_target="tpu_custom_call" | custom-call | flops 1509949440 | bytes 11796480 | tf_op jit(solution)/shard_map/expert/pallas_call | solution.py:459
  101.3 0.7 copy-done
  102.0 0.7 copy-done.1
  102.7 3.5 %all-to-all-start.3 = ((bf16[4,4,144,128]{3,2,1,0:T(8,128)(2,1)}), bf16[4,4,144,128]{3,2,1,0:T(8,128)(2,1)S(1)}, u32[]{:S(2)}, u32[]{:S(2)}) async-start(bf16[4,4,144,128]{3,2,1,0:T(8,128)(2,1)} %get-tuple-element.51), calls=%async_computation.3 | async-start | bytes 1179648 | tf_op jit(solution)/shard_map/all_to_all | solution.py:20
  106.2 3.5 %row_pack.1 = (bf16[5040,128]{1,0:T(8,128)(2,1)}, bf16[5040,128]{1,0:T(8,128)(2,1)}, bf16[432,128]{1,0:T(8,128)(2,1)}) custom-call(s32[1]{0:T(128)} %bitcast.core_ref, bf16[4,4,384,128]{3,2,1,0:T(8,128)(2,1)} %copy-done.4, bf16[144,512]{1,0:T(8,128)(2,1)} %copy-done.1, bf16[144,1024]{1,0:T(8,128)(2,1)} %copy-done), custom_call_target="tpu_custom_call" | custom-call | flops 905969664 | bytes 11796480 | tf_op jit(solution)/shard_map/row_pack/pallas_call | solution.py:484
  109.7 4.0 %all-to-all-done.3.parts_ref = bf16[4,4,144,128]{3,2,1,0:T(8,128)(2,1)S(1)} async-done(((bf16[4,4,144,128]{3,2,1,0:T(8,128)(2,1)}), bf16[4,4,144,128]{3,2,1,0:T(8,128)(2,1)S(1)}, u32[]{:S(2)}, u32[]{:S(2)}) %all-to-all-start.3) | async-done | bytes 589856 | tf_op jit(solution)/shard_map/all_to_all | solution.py:20
  113.8 7.8 %all_to_all.42.refs_0_ = bf16[4,144,128]{2,1,0:T(8,128)(2,1)S(1)} all-to-all(bf16[4,144,128]{2,1,0:T(8,128)(2,1)S(1)} %line_sum.1), channel_id=1, replica_groups={{0,1,2,3},{4,5,6,7},{8,9,10,11},{12,13,14,15},{16,20,24,28},{17,21,25,2..., dimensions={0} | all-to-all | bytes 294912 | tf_op jit(solution)/shard_map/all_to_all | solution.py:20
  121.5 0.9 spread.1
  122.5 2.2 %collective-permute-start.4 = (bf16[5040,128]{1,0:T(8,128)(2,1)}, bf16[5040,128]{1,0:T(8,128)(2,1)S(1)}, u32[]{:S(2)}, u32[]{:S(2)}) collective-permute-start(bf16[5040,128]{1,0:T(8,128)(2,1)} %get-tuple-element.61.own_ref), channel_id=1, source_target_pairs={{0,1},{16,20},{1,2},{17,21},{2,3},{18,22},{3,0},{19,23},{4,5},{20,... | collective-permute-start | bytes 3870728 | tf_op jit(solution)/shard_map/ppermute | solution.py:523
  124.7 4.3 %collective-permute-start.5 = (bf16[5040,128]{1,0:T(8,128)(2,1)}, bf16[5040,128]{1,0:T(8,128)(2,1)}, u32[]{:S(2)}, u32[]{:S(2)}) collective-permute-start(bf16[5040,128]{1,0:T(8,128)(2,1)} %get-tuple-element.62), channel_id=1, source_target_pairs={{0,3},{16,28},{1,0},{17,29},{2,1},{18,30},{3,2},{19,31},{4,7},{20,... | collective-permute-start | bytes 3870728 | tf_op jit(solution)/shard_map/ppermute | solution.py:524
  129.0 8.0 %all-to-all-start.5 = ((bf16[32,24,128]{2,1,0:T(8,128)(2,1)}), bf16[32,24,128]{2,1,0:T(8,128)(2,1)S(1)}, u32[]{:S(2)}, u32[]{:S(2)}) async-start(bf16[32,24,128]{2,1,0:T(8,128)(2,1)} %bitcast.12), calls=%async_computation.5 | async-start | bytes 393216 | tf_op jit(solution)/shard_map/all_to_all | solution.py:20
  137.0 1.0 copy.20.gain_ref
  138.2 3.1 %norm.1 = (bf16[1024,192]{1,0:T(8,128)(2,1)}, bf16[1024,192]{1,0:T(8,128)(2,1)}, bf16[1024,192]{1,0:T(8,128)(2,1)}, f32[2,192]{1,0:T(2,128)}) custom-call(s32[1]{0:T(128)} %bitcast.core_ref, bf16[4,4,384,128]{3,2,1,0:T(8,128)(2,1)} %copy-done.4, f32[1024,1]{1,0:T(8,128)} %copy.20.gain_ref), custom_call_target="tpu_custom_call" | custom-call | flops 905969664 | bytes 11796480 | tf_op jit(solution)/shard_map/norm/pallas_call | solution.py:530
  141.3 14.6 %all-to-all-done.5 = bf16[32,24,128]{2,1,0:T(8,128)(2,1)S(1)} async-done(((bf16[32,24,128]{2,1,0:T(8,128)(2,1)}), bf16[32,24,128]{2,1,0:T(8,128)(2,1)S(1)}, u32[]{:S(2)}, u32[]{:S(2)}) %all-to-all-start.5) | async-done | bytes 196640 | tf_op jit(solution)/shard_map/all_to_all | solution.py:20
  155.9 0.7 copy-done.7
  156.6 3.0 %mix.1 = (bf16[16,32,128]{2,1,0:T(8,128)(2,1)}, bf16[16,32,128]{2,1,0:T(8,128)(2,1)}, bf16[16,104,128]{2,1,0:T(8,128)(2,1)}) custom-call(s32[1]{0:T(128)} %bitcast.core_ref, bf16[768,192]{1,0:T(8,128)(2,1)} %get-tuple-element.67.refs_0_, bf16[768,128]{1,0:T(8,128)(2,1)} %bitcast.80, bf16[192,128]{1,0:T(8,128)(2,1)} %get-tuple-element.68.refs_2_, ...), custom_call_target="tpu_custom_call" | custom-call | tf_op jit(solution)/shard_map/mix/pallas_call | solution.py:559
  159.7 3.3 %collective-permute-start.9 = (bf16[16,32,128]{2,1,0:T(8,128)(2,1)}, bf16[16,32,128]{2,1,0:T(8,128)(2,1)S(1)}, u32[]{:S(2)}, u32[]{:S(2)}) collective-permute-start(bf16[16,32,128]{2,1,0:T(8,128)(2,1)} %get-tuple-element.73), channel_id=1, source_target_pairs={{0,16},{16,0},{1,17},{17,1},{2,18},{18,2},{3,19},{19,3},{4,20},{20... | collective-permute-start | bytes 393224 | tf_op jit(solution)/shard_map/ppermute | solution.py:574
  163.0 3.6 %all-to-all-start.6 = ((bf16[16,104,128]{2,1,0:T(8,128)(2,1)}), bf16[16,104,128]{2,1,0:T(8,128)(2,1)S(1)}, u32[]{:S(2)}, u32[]{:S(2)}) async-start(bf16[16,104,128]{2,1,0:T(8,128)(2,1)} %get-tuple-element.74), calls=%async_computation.6 | async-start | bytes 851968 | tf_op jit(solution)/shard_map/all_to_all | solution.py:20
  166.6 0.5 slice_bitcast_fusion.30
  167.1 1.6 add_convert_fusion
  168.7 8.1 %all-to-all-done.6.refs_0_ = bf16[16,104,128]{2,1,0:T(8,128)(2,1)S(1)} async-done(((bf16[16,104,128]{2,1,0:T(8,128)(2,1)}), bf16[16,104,128]{2,1,0:T(8,128)(2,1)S(1)}, u32[]{:S(2)}, u32[]{:S(2)}) %all-to-all-start.6) | async-done | bytes 426016 | tf_op jit(solution)/shard_map/all_to_all | solution.py:20
  176.9 3.1 %collective-permute-start.10 = (f32[64,30]{1,0:T(8,128)S(1)}, f32[64,30]{1,0:T(8,128)S(1)}, u32[]{:S(2)}, u32[]{:S(2)}) collective-permute-start(f32[64,30]{1,0:T(8,128)S(1)} %get-tuple-element.79), channel_id=1, source_target_pairs={{16,0},{32,16},{48,32},{64,48},{80,64},{96,80},{112,96},{128,112},... | collective-permute-start | bytes 23048 | tf_op jit(solution)/shard_map/ppermute | solution.py:593
  180.0 3.5 %all-to-all-start.7 = ((bf16[16,32,128]{2,1,0:T(8,128)(2,1)}), bf16[16,32,128]{2,1,0:T(8,128)(2,1)S(1)}, u32[]{:S(2)}, u32[]{:S(2)}) async-start(bf16[16,32,128]{2,1,0:T(8,128)(2,1)} %add_convert_fusion), calls=%async_computation.7 | async-start | bytes 262144 | tf_op jit(solution)/shard_map/all_to_all | solution.py:20
  183.6 1.9 collective-permute-start.6
  185.5 1.1 slice.261
  186.6 4.6 %collective-permute-start.7 = (bf16[2304,128]{1,0:T(8,128)(2,1)S(1)}, bf16[2304,128]{1,0:T(8,128)(2,1)}, u32[]{:S(2)}, u32[]{:S(2)}) collective-permute-start(bf16[2304,128]{1,0:T(8,128)(2,1)S(1)} %slice.261), channel_id=1, source_target_pairs={{0,3},{16,28},{1,0},{17,29},{2,1},{18,30},{3,2},{19,31},{4,7},{20,... | collective-permute-start | bytes 1769480 | tf_op jit(solution)/shard_map/ppermute | solution.py:528
  191.2 2.1 %collective-permute-start.8 = (bf16[432,128]{1,0:T(8,128)(2,1)}, bf16[432,128]{1,0:T(8,128)(2,1)S(1)}, u32[]{:S(2)}, u32[]{:S(2)}) collective-permute-start(bf16[432,128]{1,0:T(8,128)(2,1)} %get-tuple-element.63), channel_id=1, source_target_pairs={{0,2},{16,24},{1,3},{17,25},{2,0},{18,26},{3,1},{19,27},{4,6},{20,... | collective-permute-start | bytes 331784 | tf_op jit(solution)/shard_map/ppermute | solution.py:525
  193.4 1.8 multiply_convert_fusion
  195.2 0.6 multiply_convert_fusion.1
  196.0 0.6 convert_reduce_fusion
  196.6 2.1 %collective-permute-done.8.across_ref = bf16[432,128]{1,0:T(8,128)(2,1)S(1)} collective-permute-done((bf16[432,128]{1,0:T(8,128)(2,1)}, bf16[432,128]{1,0:T(8,128)(2,1)S(1)}, u32[]{:S(2)}, u32[]{:S(2)}) %collective-permute-start.8) | collective-permute-done | bytes 110624 | tf_op jit(solution)/shard_map/ppermute | solution.py:525
  198.8 0.5 collective-permute-done.7.high_ref
  199.4 5.5 %weight_sum.1 = (bf16[2048,128]{1,0:T(8,128)(2,1)}, bf16[2048,128]{1,0:T(8,128)(2,1)}, bf16[128,2048]{1,0:T(8,128)(2,1)}) custom-call(bf16[5040,128]{1,0:T(8,128)(2,1)} %get-tuple-element.61.own_ref, bf16[5040,128]{1,0:T(8,128)(2,1)} %copy-done.6, bf16[5040,128]{1,0:T(8,128)(2,1)} %collective-permute-done.5.ahead_ref, ...), custom_call_target="tpu_custom_call" | custom-call | flops 905969664 | bytes 11796480 | tf_op jit(solution)/shard_map/weight_sum/pallas_call | solution.py:607
  (44 shorter events, 0.8 us)
Async XLA Ops:
  3.2 10.1 %copy-start.8 = (bf16[1280,128]{1,0:T(8,128)(2,1)S(1)}, bf16[1280,128]{1,0:T(8,128)(2,1)}, u32[]{:S(2)}) copy-start(bf16[1280,128]{1,0:T(8,128)(2,1)} %get-tuple-element.43) | copy-start | bytes 983044
  3.2 51.3 %copy-start.2 = (bf16[64,192]{1,0:T(8,128)(2,1)S(1)}, bf16[64,192]{1,0:T(8,128)(2,1)}, u32[]{:S(2)}) copy-start(bf16[64,192]{1,0:T(8,128)(2,1)} %refs_1_.3) | copy-start | bytes 73732
  5.9 59.6 %collective-permute-start = (bf16[6144,128]{1,0:T(8,128)(2,1)}, bf16[6144,128]{1,0:T(8,128)(2,1)S(1)}, u32[]{:S(2)}, u32[]{:S(2)}) collective-permute-start(bf16[6144,128]{1,0:T(8,128)(2,1)} %pack.1.refs_0_), channel_id=1, source_target_pairs={{0,1},{16,20},{1,2},{17,21},{2,3},{18,22},{3,0},{19,23},{4,5},{20,... | collective-permute-start | bytes 4718600 | tf_op jit(solution)/shard_map/ppermute | solution.py:435
  10.0 55.6 %collective-permute-start.1 = (bf16[6144,128]{1,0:T(8,128)(2,1)}, bf16[6144,128]{1,0:T(8,128)(2,1)}, u32[]{:S(2)}, u32[]{:S(2)}) collective-permute-start(bf16[6144,128]{1,0:T(8,128)(2,1)} %pack.1.refs_0_), channel_id=1, source_target_pairs={{0,3},{16,28},{1,0},{17,29},{2,1},{18,30},{3,2},{19,31},{4,7},{20,... | collective-permute-start | bytes 4718600 | tf_op jit(solution)/shard_map/ppermute | solution.py:436
  65.5 5.2 %copy-start.5 = (bf16[6144,128]{1,0:T(8,128)(2,1)}, bf16[6144,128]{1,0:T(8,128)(2,1)S(1)}, u32[]{:S(2)}) copy-start(bf16[6144,128]{1,0:T(8,128)(2,1)S(1)} %collective-permute-done.refs_1_) | copy-start | bytes 4718596
  67.2 26.1 %all-to-all-start.2 = ((bf16[4,4,384,128]{3,2,1,0:T(8,128)(2,1)}), bf16[4,4,384,128]{3,2,1,0:T(8,128)(2,1)S(1)}, u32[]{:S(2)}, u32[]{:S(2)}) async-start(bf16[4,4,384,128]{3,2,1,0:T(8,128)(2,1)} %broadcast_in_dim.21), calls=%async_computation.2 | async-start | bytes 3145728 | tf_op jit(solution)/shard_map/all_to_all | solution.py:20
  71.7 21.6 %collective-permute-start.2 = (bf16[3072,128]{1,0:T(8,128)(2,1)}, bf16[3072,128]{1,0:T(8,128)(2,1)S(1)}, u32[]{:S(2)}, u32[]{:S(2)}) collective-permute-start(bf16[3072,128]{1,0:T(8,128)(2,1)} %slice.195), channel_id=1, source_target_pairs={{0,1},{16,20},{1,2},{17,21},{2,3},{18,22},{3,0},{19,23},{4,5},{20,... | collective-permute-start | bytes 2359304 | tf_op jit(solution)/shard_map/ppermute | solution.py:453
  76.0 17.3 %collective-permute-start.3 = (bf16[3072,128]{1,0:T(8,128)(2,1)}, bf16[3072,128]{1,0:T(8,128)(2,1)S(1)}, u32[]{:S(2)}, u32[]{:S(2)}) collective-permute-start(bf16[3072,128]{1,0:T(8,128)(2,1)} %slice.196), channel_id=1, source_target_pairs={{0,3},{16,28},{1,0},{17,29},{2,1},{18,30},{3,2},{19,31},{4,7},{20,... | collective-permute-start | bytes 2359304 | tf_op jit(solution)/shard_map/ppermute | solution.py:454
  93.3 1.2 copy-start.4
  101.3 0.7 copy-start
  102.0 0.7 copy-start.1
  102.7 11.0 %all-to-all-start.3 = ((bf16[4,4,144,128]{3,2,1,0:T(8,128)(2,1)}), bf16[4,4,144,128]{3,2,1,0:T(8,128)(2,1)S(1)}, u32[]{:S(2)}, u32[]{:S(2)}) async-start(bf16[4,4,144,128]{3,2,1,0:T(8,128)(2,1)} %get-tuple-element.51), calls=%async_computation.3 | async-start | bytes 1179648 | tf_op jit(solution)/shard_map/all_to_all | solution.py:20
  109.7 27.3 %copy-start.13 = (f32[1024]{0:T(1024)S(1)}, f32[1024]{0:T(1024)}, u32[]{:S(2)}) copy-start(f32[1024]{0:T(1024)} %param.25) | copy-start | bytes 12292
  122.5 61.1 %collective-permute-start.4 = (bf16[5040,128]{1,0:T(8,128)(2,1)}, bf16[5040,128]{1,0:T(8,128)(2,1)S(1)}, u32[]{:S(2)}, u32[]{:S(2)}) collective-permute-start(bf16[5040,128]{1,0:T(8,128)(2,1)} %get-tuple-element.61.own_ref), channel_id=1, source_target_pairs={{0,1},{16,20},{1,2},{17,21},{2,3},{18,22},{3,0},{19,23},{4,5},{20,... | collective-permute-start | bytes 3870728 | tf_op jit(solution)/shard_map/ppermute | solution.py:523
  124.7 60.9 %collective-permute-start.5 = (bf16[5040,128]{1,0:T(8,128)(2,1)}, bf16[5040,128]{1,0:T(8,128)(2,1)}, u32[]{:S(2)}, u32[]{:S(2)}) collective-permute-start(bf16[5040,128]{1,0:T(8,128)(2,1)} %get-tuple-element.62), channel_id=1, source_target_pairs={{0,3},{16,28},{1,0},{17,29},{2,1},{18,30},{3,2},{19,31},{4,7},{20,... | collective-permute-start | bytes 3870728 | tf_op jit(solution)/shard_map/ppermute | solution.py:524
  129.0 27.0 %all-to-all-start.5 = ((bf16[32,24,128]{2,1,0:T(8,128)(2,1)}), bf16[32,24,128]{2,1,0:T(8,128)(2,1)S(1)}, u32[]{:S(2)}, u32[]{:S(2)}) async-start(bf16[32,24,128]{2,1,0:T(8,128)(2,1)} %bitcast.12), calls=%async_computation.5 | async-start | bytes 393216 | tf_op jit(solution)/shard_map/all_to_all | solution.py:20
  155.9 0.7 copy-start.7
  156.6 9.9 %copy-start.12 = (f32[64,31]{0,1:T(8,128)S(1)}, f32[64,31]{0,1:T(8,128)}, u32[]{:S(2)}) copy-start(f32[64,31]{0,1:T(8,128)} %param.23) | copy-start | bytes 23812
  156.6 20.1 %copy-start.3 = (f32[2,192]{1,0:T(2,128)S(1)}, f32[2,192]{1,0:T(2,128)}, u32[]{:S(2)}) copy-start(f32[2,192]{1,0:T(2,128)} %get-tuple-element.77.refs_3_) | copy-start | bytes 4612
  159.7 7.4 %collective-permute-start.9 = (bf16[16,32,128]{2,1,0:T(8,128)(2,1)}, bf16[16,32,128]{2,1,0:T(8,128)(2,1)S(1)}, u32[]{:S(2)}, u32[]{:S(2)}) collective-permute-start(bf16[16,32,128]{2,1,0:T(8,128)(2,1)} %get-tuple-element.73), channel_id=1, source_target_pairs={{0,16},{16,0},{1,17},{17,1},{2,18},{18,2},{3,19},{19,3},{4,20},{20... | collective-permute-start | bytes 393224 | tf_op jit(solution)/shard_map/ppermute | solution.py:574
  163.0 13.8 %all-to-all-start.6 = ((bf16[16,104,128]{2,1,0:T(8,128)(2,1)}), bf16[16,104,128]{2,1,0:T(8,128)(2,1)S(1)}, u32[]{:S(2)}, u32[]{:S(2)}) async-start(bf16[16,104,128]{2,1,0:T(8,128)(2,1)} %get-tuple-element.74), calls=%async_computation.6 | async-start | bytes 851968 | tf_op jit(solution)/shard_map/all_to_all | solution.py:20
  176.8 16.6 %copy-start.9 = (bf16[64,192]{1,0:T(8,128)(2,1)S(1)}, bf16[64,192]{1,0:T(8,128)(2,1)}, u32[]{:S(2)}) copy-start(bf16[64,192]{1,0:T(8,128)(2,1)} %param.22) | copy-start | bytes 73732
  176.8 16.6 %copy-start.11 = (bf16[64,192]{1,0:T(8,128)(2,1)S(1)}, bf16[64,192]{1,0:T(8,128)(2,1)}, u32[]{:S(2)}) copy-start(bf16[64,192]{1,0:T(8,128)(2,1)} %param.21) | copy-start | bytes 73732
  176.9 16.5 %copy-start.14 = (f32[64]{0:T(128)S(1)}, f32[64]{0:T(128)}, u32[]{:S(2)}) copy-start(f32[64]{0:T(128)} %get-tuple-element.99) | copy-start | bytes 772
  176.9 16.5 %copy-start.15 = (f32[64]{0:T(128)S(1)}, f32[64]{0:T(128)}, u32[]{:S(2)}) copy-start(f32[64]{0:T(128)} %get-tuple-element.100) | copy-start | bytes 772
  176.9 16.4 %collective-permute-start.10 = (f32[64,30]{1,0:T(8,128)S(1)}, f32[64,30]{1,0:T(8,128)S(1)}, u32[]{:S(2)}, u32[]{:S(2)}) collective-permute-start(f32[64,30]{1,0:T(8,128)S(1)} %get-tuple-element.79), channel_id=1, source_target_pairs={{16,0},{32,16},{48,32},{64,48},{80,64},{96,80},{112,96},{128,112},... | collective-permute-start | bytes 23048 | tf_op jit(solution)/shard_map/ppermute | solution.py:593
  180.0 16.0 %all-to-all-start.7 = ((bf16[16,32,128]{2,1,0:T(8,128)(2,1)}), bf16[16,32,128]{2,1,0:T(8,128)(2,1)S(1)}, u32[]{:S(2)}, u32[]{:S(2)}) async-start(bf16[16,32,128]{2,1,0:T(8,128)(2,1)} %add_convert_fusion), calls=%async_computation.7 | async-start | bytes 262144 | tf_op jit(solution)/shard_map/all_to_all | solution.py:20
  183.5 15.7 %copy-start.6 = (bf16[5040,128]{1,0:T(8,128)(2,1)}, bf16[5040,128]{1,0:T(8,128)(2,1)S(1)}, u32[]{:S(2)}) copy-start(bf16[5040,128]{1,0:T(8,128)(2,1)S(1)} %collective-permute-done.4.behind_ref) | copy-start | bytes 3870724
  183.6 15.2 %collective-permute-start.6 = (bf16[2304,128]{1,0:T(8,128)(2,1)S(1)}, bf16[2304,128]{1,0:T(8,128)(2,1)}, u32[]{:S(2)}, u32[]{:S(2)}) collective-permute-start(bf16[2304,128]{1,0:T(8,128)(2,1)S(1)} %slice.260), channel_id=1, source_target_pairs={{0,1},{16,20},{1,2},{17,21},{2,3},{18,22},{3,0},{19,23},{4,5},{20,... | collective-permute-start | bytes 1769480 | tf_op jit(solution)/shard_map/ppermute | solution.py:527
  186.6 12.6 %collective-permute-start.7 = (bf16[2304,128]{1,0:T(8,128)(2,1)S(1)}, bf16[2304,128]{1,0:T(8,128)(2,1)}, u32[]{:S(2)}, u32[]{:S(2)}) collective-permute-start(bf16[2304,128]{1,0:T(8,128)(2,1)S(1)} %slice.261), channel_id=1, source_target_pairs={{0,3},{16,28},{1,0},{17,29},{2,1},{18,30},{3,2},{19,31},{4,7},{20,... | collective-permute-start | bytes 1769480 | tf_op jit(solution)/shard_map/ppermute | solution.py:528
  191.2 7.5 %collective-permute-start.8 = (bf16[432,128]{1,0:T(8,128)(2,1)}, bf16[432,128]{1,0:T(8,128)(2,1)S(1)}, u32[]{:S(2)}, u32[]{:S(2)}) collective-permute-start(bf16[432,128]{1,0:T(8,128)(2,1)} %get-tuple-element.63), channel_id=1, source_target_pairs={{0,2},{16,24},{1,3},{17,25},{2,0},{18,26},{3,1},{19,27},{4,6},{20,... | collective-permute-start | bytes 331784 | tf_op jit(solution)/shard_map/ppermute | solution.py:525
  198.7 0.6 copy-start.10
where the time goes:
time: 207 us; the launch traced here: 205 us
  blocking collectives  59.5 us (29%)
  starting transfers between devices  57.4 us (28%)
  waiting for transfers between devices  42.5 us (21%)
  Pallas kernels  28.9 us (14%)
  local copies, waits for them, and re-layouts  11 us (5%)
  other arithmetic  4.64 us (2%)
    all_to_all x3, blocking collectives, exchanged(): lax.all_to_all(blocks, axis, 0, 0, axis_index_groups=index_groups, tiled=...  59.5 us
    all_to_all x5, waiting for transfers between devices, exchanged(): lax.all_to_all(blocks, axis, 0, 0, axis_index_groups=index_groups, tiled=...  27 us
    all_to_all x5, starting transfers between devices, exchanged(): lax.all_to_all(blocks, axis, 0, 0, axis_index_groups=index_groups, tiled=...  22.1 us
    ppermute x1, waiting for transfers between devices, body(): lax.ppermute(weights[1][:middle], PLANE, onward)  13 us
    pallas_call x1, Pallas kernels, body(): pl.pallas_call(expert_kernel, in_specs=[scalar(), whole()] + [hbm] * 5, o...  6.84 us
    pallas_call x1, Pallas kernels, body(): pl.pallas_call(weight_kernel, in_specs=[whole()] * 8, out_specs=[whole()]...  5.5 us
    ppermute x1, starting transfers between devices, body(): far_high = lax.ppermute(from_ahead[far_rows:2 * far_rows], PLANE, backward)  4.57 us
    ppermute x1, starting transfers between devices, body(): from_ahead = lax.ppermute(to_backward, PLANE, backward)  4.3 us
  transfers between devices with their start and end apart: 16, of which 7 were waited for; matrix products, arithmetic and copies ran while one was open for 5% of the time, Pallas kernels for 5%

commit v1 on v0

--- a/solution.py
+++ b/solution.py
@@ -160,15 +160,15 @@
         out_ref[pl.ds(2 * height + k * width, width), :] = down_ref[:, pl.ds(k * width, width)]
 
 
-def expert_kernel(core_ref, rows_ref, *refs):
+def expert_kernel(core_ref, rows_hbm, *refs):
     weights_hbm = refs[0:5]
-    back_ref, hidden_ref, both_ref = refs[5:8]
-    weights, acc_ref, sems = refs[8:12], refs[12], refs[13]
+    back_ref, hidden_ref, both_ref, rows_ref = refs[5:9]
+    weights, acc_ref, sems = refs[9:13], refs[13], refs[14]
     middle = weights_hbm[3].shape[0]
-    targets = (*weights[:3], weights[3].at[pl.ds(0, middle)], weights[3].at[pl.ds(middle, middle)])
+    targets = (rows_ref, *weights[:3], weights[3].at[pl.ds(0, middle)], weights[3].at[pl.ds(middle, middle)])
     copies = [
         pltpu.make_async_copy(source, target, sems.at[i])
-        for i, (source, target) in enumerate(zip(weights_hbm, targets, strict=True))
+        for i, (source, target) in enumerate(zip((rows_hbm, *weights_hbm), targets, strict=True))
     ]
     for copy in copies:
         copy.start()
@@ -176,12 +176,13 @@
     count = hidden_ref.shape[0]
     pieces = pieces_of(core_ref, ny, nx)
     height = ny * nx * width
+    copies[0].wait()
     x = jnp.concatenate([rows_ref[a, b, pl.ds(0, count), :] for a, b in pieces], axis=1)
     g = jnp.concatenate([rows_ref[a, b, pl.ds(count, count), :] for a, b in pieces], axis=1)
     for k, block in enumerate(weights):
-        copies[k].wait()
+        copies[1 + k].wait()
         if k == 3:
-            copies[4].wait()
+            copies[5].wait()
         w_both = jnp.concatenate([block[pl.ds(0, height), :], block[pl.ds(height, height), :]], axis=1)
         w_down = jnp.concatenate(
             [block[pl.ds(2 * height + i * width, width), :] for i in range(ny * nx)], axis=1
@@ -447,7 +448,8 @@
         compiler_params=params(16),
         name="compact",
     )(part.reshape(groups * pitch, width), norm_input)
-    quarters, *weights = lax.optimization_barrier((exchanged(quarters, PLANE, first_groups), *weights))
+    quarters = exchanged(quarters, PLANE, first_groups)
+    weights = list(weights)
     middle = weights[0].shape[0] // 2
     weights += [
         lax.ppermute(weights[1][:middle], PLANE, onward),
@@ -458,7 +460,7 @@
     packed_weights = pltpu.VMEM((3 * model_width, ff), bf16)
     back, hidden, both = pl.pallas_call(
         expert_kernel,
-        in_specs=[scalar(), whole()] + [hbm] * 5,
+        in_specs=[scalar()] + [hbm] * 6,
         out_specs=[whole()] * 3,
         out_shape=[
             struct((ny, nx, quarter, width), bf16),
@@ -466,14 +468,15 @@
             struct((quarter, 2 * nx * ff), bf16),
         ],
         scratch_shapes=[
+            pltpu.VMEM((ny, nx, rows_height, width), bf16),
             packed_weights,
             packed_weights,
             packed_weights,
             packed_weights,
             pltpu.VMEM((quarter, model_width), f32),
-            pltpu.SemaphoreType.DMA((5,)),
+            pltpu.SemaphoreType.DMA((6,)),
         ],
-        compiler_params=params(50),
+        compiler_params=params(58),
         cost_estimate=cost(10 * total * model_width * ff, 10 * total * model_width),
         name="expert",
     )(core, gathered, *weights)

time: 207 us -> 197 us (0.952)
  blocking collectives: 59.5 us -> 17.8 us
  starting transfers between devices: 57.4 us -> 74.9 us
  waiting for transfers between devices: 42.5 us -> 59.4 us
  local copies, waits for them, and re-layouts: 11 us -> 8.59 us
    all_to_all x3 -> x2, blocking collectives: 59.5 us -> 17.8 us  [exchanged(): lax.all_to_all(blocks, axis, 0, 0, axis_index_groups=index_groups, tiled=...]
    all_to_all x5 -> x6, starting transfers between devices: 22.1 us -> 40.3 us  [exchanged(): lax.all_to_all(blocks, axis, 0, 0, axis_index_groups=index_groups, tiled=...]
    all_to_all x5 -> x6, waiting for transfers between devices: 27 us -> 42.3 us  [exchanged(): lax.all_to_all(blocks, axis, 0, 0, axis_index_groups=index_groups, tiled=...]
  transfers between devices with their start and end apart: 16 -> 17, of which waited for: 7 -> 7; matrix products, arithmetic and copies ran while one was open for 5% -> 6% of each run, Pallas kernels for 5% -> 7%
where the time goes in v1:
time: 197 us; the launch traced here: 195 us
  starting transfers between devices  74.9 us (38%)
  waiting for transfers between devices  59.4 us (30%)
  Pallas kernels  27.8 us (14%)
  blocking collectives  17.8 us (9%)
  local copies, waits for them, and re-layouts  8.59 us (4%)
  other arithmetic  5.47 us (3%)
    all_to_all x6, waiting for transfers between devices, exchanged(): lax.all_to_all(blocks, axis, 0, 0, axis_index_groups=index_groups, tiled=...  42.3 us
    all_to_all x6, starting transfers between devices, exchanged(): lax.all_to_all(blocks, axis, 0, 0, axis_index_groups=index_groups, tiled=...  40.3 us
    all_to_all x2, blocking collectives, exchanged(): lax.all_to_all(blocks, axis, 0, 0, axis_index_groups=index_groups, tiled=...  17.8 us
    ppermute x1, waiting for transfers between devices, body(): lax.ppermute(weights[1][:middle], PLANE, onward)  14.8 us
    pallas_call x1, Pallas kernels, body(): pl.pallas_call(expert_kernel, in_specs=[scalar()] + [hbm] * 6, out_specs=...  5.96 us
    pallas_call x1, Pallas kernels, body(): pl.pallas_call(weight_kernel, in_specs=[whole()] * 8, out_specs=[whole()]...  5.5 us
    ppermute x1, starting transfers between devices, body(): far_high = lax.ppermute(from_ahead[far_rows:2 * far_rows], PLANE, backward)  4.56 us
    ppermute x1, starting transfers between devices, body(): from_ahead = lax.ppermute(to_backward, PLANE, backward)  4.3 us
  transfers between devices with their start and end apart: 17, of which 7 were waited for; matrix products, arithmetic and copies ran while one was open for 6% of the time, Pallas kernels for 7%

profile of v1, /device:TPU:1, one launch (start us, length us, event | category | flops | bytes accessed | tf_op | source)
XLA Modules:
  0.0 194.9 jit_solution(4215962881025228161)
XLA Ops:
  0.6 2.6 %prep.1 = (bf16[1280,128]{1,0:T(8,128)(2,1)}, bf16[768,192]{1,0:T(8,128)(2,1)}, bf16[192,128]{1,0:T(8,128)(2,1)}) custom-call(s32[1]{0:T(128)} %bitcast.1.refs_0_, s32[2,192]{1,0:T(2,128)} %bitcast.83, f32[2,192]{1,0:T(2,128)} %bitcast.84, bf16[192,2048]{1,0:T(8,128)(2,1)} %refs_3_.2, bf16[192,2048]{1,0:T(8,128)(2,1)} %refs_4_.1), custom_call_target="tpu_custom_call" | custom-call | tf_op jit(solution)/shard_map/prep/pallas_call | solution.py:397
  3.2 16.7 %all-to-all-start = ((bf16[32,40,128]{2,1,0:T(8,128)(2,1)}), bf16[32,40,128]{2,1,0:T(8,128)(2,1)S(1)}, u32[]{:S(2)}, u32[]{:S(2)}) async-start(bf16[32,40,128]{2,1,0:T(8,128)(2,1)} %bitcast.81), calls=%async_computation | async-start | bytes 655360 | tf_op jit(solution)/shard_map/all_to_all | solution.py:20
  20.0 2.7 %pack.1.refs_0_ = bf16[6144,128]{1,0:T(8,128)(2,1)} custom-call(bf16[2048,128]{1,0:T(8,128)(2,1)} %bitcast.85, bf16[2048,128]{1,0:T(8,128)(2,1)} %bitcast.86, bf16[128,2048]{1,0:T(8,128)(2,1)} %bitcast.87), custom_call_target="tpu_custom_call" | custom-call | flops 1207959552 | bytes 1572864 | tf_op jit(solution)/shard_map/pack/pallas_call | solution.py:424
  22.6 3.2 %collective-permute-start = (bf16[6144,128]{1,0:T(8,128)(2,1)}, bf16[6144,128]{1,0:T(8,128)(2,1)}, u32[]{:S(2)}, u32[]{:S(2)}) collective-permute-start(bf16[6144,128]{1,0:T(8,128)(2,1)} %pack.1.refs_0_), channel_id=1, source_target_pairs={{0,1},{16,20},{1,2},{17,21},{2,3},{18,22},{3,0},{19,23},{4,5},{20,... | collective-permute-start | bytes 4718600 | tf_op jit(solution)/shard_map/ppermute | solution.py:436
  25.8 3.4 %collective-permute-start.1 = (bf16[6144,128]{1,0:T(8,128)(2,1)}, bf16[6144,128]{1,0:T(8,128)(2,1)}, u32[]{:S(2)}, u32[]{:S(2)}) collective-permute-start(bf16[6144,128]{1,0:T(8,128)(2,1)} %pack.1.refs_0_), channel_id=1, source_target_pairs={{0,3},{16,28},{1,0},{17,29},{2,1},{18,30},{3,2},{19,31},{4,7},{20,... | collective-permute-start | bytes 4718600 | tf_op jit(solution)/shard_map/ppermute | solution.py:437
  29.2 15.7 %all-to-all-done = bf16[32,40,128]{2,1,0:T(8,128)(2,1)S(1)} async-done(((bf16[32,40,128]{2,1,0:T(8,128)(2,1)}), bf16[32,40,128]{2,1,0:T(8,128)(2,1)S(1)}, u32[]{:S(2)}, u32[]{:S(2)}) %all-to-all-start) | async-done | bytes 327712 | tf_op jit(solution)/shard_map/all_to_all | solution.py:20
  44.9 0.5 compact.1
  45.4 10.4 %all_to_all.40 = bf16[4,384,128]{2,1,0:T(8,128)(2,1)S(1)} all-to-all(bf16[4,384,128]{2,1,0:T(8,128)(2,1)S(1)} %compact.1), channel_id=1, replica_groups={{0,1,2,3},{4,5,6,7},{8,9,10,11},{12,13,14,15},{16,20,24,28},{17,21,25,2..., dimensions={0} | all-to-all | bytes 786432 | tf_op jit(solution)/shard_map/all_to_all | solution.py:20
  55.8 1.5 broadcast_in_dim.21
  57.3 3.8 %all-to-all-start.2 = ((bf16[4,4,384,128]{3,2,1,0:T(8,128)(2,1)}), bf16[4,4,384,128]{3,2,1,0:T(8,128)(2,1)S(1)}, u32[]{:S(2)}, u32[]{:S(2)}) async-start(bf16[4,4,384,128]{3,2,1,0:T(8,128)(2,1)} %broadcast_in_dim.21), calls=%async_computation.2 | async-start | bytes 3145728 | tf_op jit(solution)/shard_map/all_to_all | solution.py:20
  61.1 1.2 slice.260
  62.3 2.2 %collective-permute-start.2 = (bf16[3072,128]{1,0:T(8,128)(2,1)S(1)}, bf16[3072,128]{1,0:T(8,128)(2,1)}, u32[]{:S(2)}, u32[]{:S(2)}) collective-permute-start(bf16[3072,128]{1,0:T(8,128)(2,1)S(1)} %slice.260), channel_id=1, source_target_pairs={{0,1},{16,20},{1,2},{17,21},{2,3},{18,22},{3,0},{19,23},{4,5},{20,... | collective-permute-start | bytes 2359304 | tf_op jit(solution)/shard_map/ppermute | solution.py:455
  64.6 1.2 slice.261
  65.8 4.3 %collective-permute-start.3 = (bf16[3072,128]{1,0:T(8,128)(2,1)S(1)}, bf16[3072,128]{1,0:T(8,128)(2,1)}, u32[]{:S(2)}, u32[]{:S(2)}) collective-permute-start(bf16[3072,128]{1,0:T(8,128)(2,1)S(1)} %slice.261), channel_id=1, source_target_pairs={{0,3},{16,28},{1,0},{17,29},{2,1},{18,30},{3,2},{19,31},{4,7},{20,... | collective-permute-start | bytes 2359304 | tf_op jit(solution)/shard_map/ppermute | solution.py:456
  70.0 14.8 %collective-permute-done.2.refs_3_ = bf16[3072,128]{1,0:T(8,128)(2,1)} collective-permute-done((bf16[3072,128]{1,0:T(8,128)(2,1)S(1)}, bf16[3072,128]{1,0:T(8,128)(2,1)}, u32[]{:S(2)}, u32[]{:S(2)}) %collective-permute-start.2) | collective-permute-done | bytes 786464 | tf_op jit(solution)/shard_map/ppermute | solution.py:455
  84.8 1.2 copy-done.2
  86.0 6.0 %expert.1 = (bf16[4,4,144,128]{3,2,1,0:T(8,128)(2,1)}, bf16[144,512]{1,0:T(8,128)(2,1)}, bf16[144,1024]{1,0:T(8,128)(2,1)}) custom-call(s32[1]{0:T(128)} %bitcast.core_ref, bf16[4,4,384,128]{3,2,1,0:T(8,128)(2,1)} %copy-done.2, bf16[6144,128]{1,0:T(8,128)(2,1)} %pack.1.refs_0_, bf16[6144,128]{1,0:T(8,128)(2,1)} %collective-permute-done.refs_1_, ...), custom_call_target="tpu_custom_call" | custom-call | flops 1509949440 | bytes 11796480 | tf_op jit(solution)/shard_map/expert/pallas_call | solution.py:461
  92.0 3.5 %all-to-all-start.3 = ((bf16[4,4,144,128]{3,2,1,0:T(8,128)(2,1)}), bf16[4,4,144,128]{3,2,1,0:T(8,128)(2,1)S(1)}, u32[]{:S(2)}, u32[]{:S(2)}) async-start(bf16[4,4,144,128]{3,2,1,0:T(8,128)(2,1)} %get-tuple-element.43), calls=%async_computation.3 | async-start | bytes 1179648 | tf_op jit(solution)/shard_map/all_to_all | solution.py:20
  95.5 3.4 %row_pack.1 = (bf16[5040,128]{1,0:T(8,128)(2,1)}, bf16[5040,128]{1,0:T(8,128)(2,1)}, bf16[432,128]{1,0:T(8,128)(2,1)}) custom-call(s32[1]{0:T(128)} %bitcast.core_ref, bf16[4,4,384,128]{3,2,1,0:T(8,128)(2,1)} %copy-done.2, bf16[144,512]{1,0:T(8,128)(2,1)} %get-tuple-element.44.hidden_ref, bf16[144,1024]{1,0:T(8,128)(2,1)} %get-tuple-element.45.both_ref), custom_call_target="tpu_custom_call" | custom-call | flops 905969664 | bytes 11796480 | tf_op jit(solution)/shard_map/row_pack/pallas_call | solution.py:487
  98.9 4.1 %all-to-all-done.3.parts_ref = bf16[4,4,144,128]{3,2,1,0:T(8,128)(2,1)S(1)} async-done(((bf16[4,4,144,128]{3,2,1,0:T(8,128)(2,1)}), bf16[4,4,144,128]{3,2,1,0:T(8,128)(2,1)S(1)}, u32[]{:S(2)}, u32[]{:S(2)}) %all-to-all-start.3) | async-done | bytes 589856 | tf_op jit(solution)/shard_map/all_to_all | solution.py:20
  103.1 7.4 %all_to_all.41.refs_0_ = bf16[4,144,128]{2,1,0:T(8,128)(2,1)S(1)} all-to-all(bf16[4,144,128]{2,1,0:T(8,128)(2,1)S(1)} %line_sum.1), channel_id=1, replica_groups={{0,1,2,3},{4,5,6,7},{8,9,10,11},{12,13,14,15},{16,20,24,28},{17,21,25,2..., dimensions={0} | all-to-all | bytes 294912 | tf_op jit(solution)/shard_map/all_to_all | solution.py:20
  110.5 0.9 spread.1
  111.4 2.2 %collective-permute-start.4 = (bf16[5040,128]{1,0:T(8,128)(2,1)}, bf16[5040,128]{1,0:T(8,128)(2,1)S(1)}, u32[]{:S(2)}, u32[]{:S(2)}) collective-permute-start(bf16[5040,128]{1,0:T(8,128)(2,1)} %get-tuple-element.53.own_ref), channel_id=1, source_target_pairs={{0,1},{16,20},{1,2},{17,21},{2,3},{18,22},{3,0},{19,23},{4,5},{20,... | collective-permute-start | bytes 3870728 | tf_op jit(solution)/shard_map/ppermute | solution.py:526
  113.6 4.3 %collective-permute-start.5 = (bf16[5040,128]{1,0:T(8,128)(2,1)}, bf16[5040,128]{1,0:T(8,128)(2,1)S(1)}, u32[]{:S(2)}, u32[]{:S(2)}) collective-permute-start(bf16[5040,128]{1,0:T(8,128)(2,1)} %get-tuple-element.54), channel_id=1, source_target_pairs={{0,3},{16,28},{1,0},{17,29},{2,1},{18,30},{3,2},{19,31},{4,7},{20,... | collective-permute-start | bytes 3870728 | tf_op jit(solution)/shard_map/ppermute | solution.py:527
  117.9 9.2 %all-to-all-start.5 = ((bf16[32,24,128]{2,1,0:T(8,128)(2,1)}), bf16[32,24,128]{2,1,0:T(8,128)(2,1)S(1)}, u32[]{:S(2)}, u32[]{:S(2)}) async-start(bf16[32,24,128]{2,1,0:T(8,128)(2,1)} %bitcast.12), calls=%async_computation.5 | async-start | bytes 393216 | tf_op jit(solution)/shard_map/all_to_all | solution.py:20
  127.1 1.0 copy.20.gain_ref
  128.3 3.1 %norm.1 = (bf16[1024,192]{1,0:T(8,128)(2,1)}, bf16[1024,192]{1,0:T(8,128)(2,1)}, bf16[1024,192]{1,0:T(8,128)(2,1)}, f32[2,192]{1,0:T(2,128)}) custom-call(s32[1]{0:T(128)} %bitcast.core_ref, bf16[4,4,384,128]{3,2,1,0:T(8,128)(2,1)} %copy-done.2, f32[1024,1]{1,0:T(8,128)} %copy.20.gain_ref), custom_call_target="tpu_custom_call" | custom-call | flops 905969664 | bytes 11796480 | tf_op jit(solution)/shard_map/norm/pallas_call | solution.py:533
  131.5 14.5 %all-to-all-done.5 = bf16[32,24,128]{2,1,0:T(8,128)(2,1)S(1)} async-done(((bf16[32,24,128]{2,1,0:T(8,128)(2,1)}), bf16[32,24,128]{2,1,0:T(8,128)(2,1)S(1)}, u32[]{:S(2)}, u32[]{:S(2)}) %all-to-all-start.5) | async-done | bytes 196640 | tf_op jit(solution)/shard_map/all_to_all | solution.py:20
  145.9 0.7 copy-done.5
  146.6 3.1 %mix.1 = (bf16[16,32,128]{2,1,0:T(8,128)(2,1)}, bf16[16,32,128]{2,1,0:T(8,128)(2,1)}, bf16[16,104,128]{2,1,0:T(8,128)(2,1)}) custom-call(s32[1]{0:T(128)} %bitcast.core_ref, bf16[768,192]{1,0:T(8,128)(2,1)} %get-tuple-element.59.refs_0_, bf16[768,128]{1,0:T(8,128)(2,1)} %bitcast.80, bf16[192,128]{1,0:T(8,128)(2,1)} %get-tuple-element.60.refs_2_, ...), custom_call_target="tpu_custom_call" | custom-call | tf_op jit(solution)/shard_map/mix/pallas_call | solution.py:562
  149.7 3.4 %collective-permute-start.9 = (bf16[16,32,128]{2,1,0:T(8,128)(2,1)}, bf16[16,32,128]{2,1,0:T(8,128)(2,1)S(1)}, u32[]{:S(2)}, u32[]{:S(2)}) collective-permute-start(bf16[16,32,128]{2,1,0:T(8,128)(2,1)} %get-tuple-element.65), channel_id=1, source_target_pairs={{0,16},{16,0},{1,17},{17,1},{2,18},{18,2},{3,19},{19,3},{4,20},{20... | collective-permute-start | bytes 393224 | tf_op jit(solution)/shard_map/ppermute | solution.py:577
  153.0 3.6 %all-to-all-start.6 = ((bf16[16,104,128]{2,1,0:T(8,128)(2,1)}), bf16[16,104,128]{2,1,0:T(8,128)(2,1)S(1)}, u32[]{:S(2)}, u32[]{:S(2)}) async-start(bf16[16,104,128]{2,1,0:T(8,128)(2,1)} %get-tuple-element.66), calls=%async_computation.6 | async-start | bytes 851968 | tf_op jit(solution)/shard_map/all_to_all | solution.py:20
  156.6 0.7 slice_bitcast_fusion.30
  157.3 1.6 add_convert_fusion
  158.9 7.9 %all-to-all-done.6.refs_0_ = bf16[16,104,128]{2,1,0:T(8,128)(2,1)S(1)} async-done(((bf16[16,104,128]{2,1,0:T(8,128)(2,1)}), bf16[16,104,128]{2,1,0:T(8,128)(2,1)S(1)}, u32[]{:S(2)}, u32[]{:S(2)}) %all-to-all-start.6) | async-done | bytes 426016 | tf_op jit(solution)/shard_map/all_to_all | solution.py:20
  166.8 3.5 %all-to-all-start.7 = ((bf16[16,32,128]{2,1,0:T(8,128)(2,1)}), bf16[16,32,128]{2,1,0:T(8,128)(2,1)S(1)}, u32[]{:S(2)}, u32[]{:S(2)}) async-start(bf16[16,32,128]{2,1,0:T(8,128)(2,1)} %add_convert_fusion), calls=%async_computation.7 | async-start | bytes 262144 | tf_op jit(solution)/shard_map/all_to_all | solution.py:20
  170.4 0.1 conv_grad.1
  170.5 3.1 %collective-permute-start.10 = (f32[64,30]{1,0:T(8,128)S(1)}, f32[64,30]{1,0:T(8,128)S(1)}, u32[]{:S(2)}, u32[]{:S(2)}) collective-permute-start(f32[64,30]{1,0:T(8,128)S(1)} %get-tuple-element.71), channel_id=1, source_target_pairs={{16,0},{32,16},{48,32},{64,48},{80,64},{96,80},{112,96},{128,112},... | collective-permute-start | bytes 23048 | tf_op jit(solution)/shard_map/ppermute | solution.py:596
  173.6 1.9 collective-permute-start.6
  175.6 0.9 slice.263
  176.5 4.6 %collective-permute-start.7 = (bf16[2304,128]{1,0:T(8,128)(2,1)}, bf16[2304,128]{1,0:T(8,128)(2,1)}, u32[]{:S(2)}, u32[]{:S(2)}) collective-permute-start(bf16[2304,128]{1,0:T(8,128)(2,1)} %slice.263), channel_id=1, source_target_pairs={{0,3},{16,28},{1,0},{17,29},{2,1},{18,30},{3,2},{19,31},{4,7},{20,... | collective-permute-start | bytes 1769480 | tf_op jit(solution)/shard_map/ppermute | solution.py:531
  181.1 2.1 %collective-permute-start.8 = (bf16[432,128]{1,0:T(8,128)(2,1)}, bf16[432,128]{1,0:T(8,128)(2,1)S(1)}, u32[]{:S(2)}, u32[]{:S(2)}) collective-permute-start(bf16[432,128]{1,0:T(8,128)(2,1)} %get-tuple-element.55), channel_id=1, source_target_pairs={{0,2},{16,24},{1,3},{17,25},{2,0},{18,26},{3,1},{19,27},{4,6},{20,... | collective-permute-start | bytes 331784 | tf_op jit(solution)/shard_map/ppermute | solution.py:528
  183.2 2.6 %multiply_convert_fusion = (bf16[64,192]{1,0:T(8,128)(2,1)}, f32[64,192]{1,0:T(8,128)S(1)}) fusion(bf16[64,192]{1,0:T(8,128)(2,1)} %param.21, bf16[64,192]{1,0:T(8,128)(2,1)S(1)} %copy-done.6, f32[64,192]{1,0:T(8,128)S(1)} %get-tuple-element.70, f32[64]{0:T(128)S(1)} %get-tuple-element.103, f32[64,30]{1,0:T(8,128)S(1)} %collective-permute-done.10, ...), kind=kLoop, calls=%fused_computation.129 | loop fusion | flops 1241088 | bytes 187648 | tf_op jit(solution)/shard_map/convert_element_type | solution.py:609
  185.8 0.6 multiply_convert_fusion.1
  186.5 0.6 convert_reduce_fusion
  187.1 1.5 collective-permute-done.8.across_ref
  188.6 0.8 collective-permute-done.7.high_ref
  189.4 5.5 %weight_sum.1 = (bf16[2048,128]{1,0:T(8,128)(2,1)}, bf16[2048,128]{1,0:T(8,128)(2,1)}, bf16[128,2048]{1,0:T(8,128)(2,1)}) custom-call(bf16[5040,128]{1,0:T(8,128)(2,1)} %get-tuple-element.53.own_ref, bf16[5040,128]{1,0:T(8,128)(2,1)} %copy-done.3, bf16[5040,128]{1,0:T(8,128)(2,1)} %copy-done.4, bf16[2304,128]{1,0:T(8,128)(2,1)} %collective-permute-done.6.low_ref, ...), custom_call_target="tpu_custom_call" | custom-call | flops 905969664 | bytes 11796480 | tf_op jit(solution)/shard_map/weight_sum/pallas_call | solution.py:610
  (33 shorter events, 0.4 us)
Async XLA Ops:
  3.2 41.7 %all-to-all-start = ((bf16[32,40,128]{2,1,0:T(8,128)(2,1)}), bf16[32,40,128]{2,1,0:T(8,128)(2,1)S(1)}, u32[]{:S(2)}, u32[]{:S(2)}) async-start(bf16[32,40,128]{2,1,0:T(8,128)(2,1)} %bitcast.81), calls=%async_computation | async-start | bytes 655360 | tf_op jit(solution)/shard_map/all_to_all | solution.py:20
  20.0 25.0 %copy-start = (bf16[64,192]{1,0:T(8,128)(2,1)S(1)}, bf16[64,192]{1,0:T(8,128)(2,1)}, u32[]{:S(2)}) copy-start(bf16[64,192]{1,0:T(8,128)(2,1)} %refs_1_.3) | copy-start | bytes 73732
  22.6 38.5 %collective-permute-start = (bf16[6144,128]{1,0:T(8,128)(2,1)}, bf16[6144,128]{1,0:T(8,128)(2,1)}, u32[]{:S(2)}, u32[]{:S(2)}) collective-permute-start(bf16[6144,128]{1,0:T(8,128)(2,1)} %pack.1.refs_0_), channel_id=1, source_target_pairs={{0,1},{16,20},{1,2},{17,21},{2,3},{18,22},{3,0},{19,23},{4,5},{20,... | collective-permute-start | bytes 4718600 | tf_op jit(solution)/shard_map/ppermute | solution.py:436
  25.8 38.7 %collective-permute-start.1 = (bf16[6144,128]{1,0:T(8,128)(2,1)}, bf16[6144,128]{1,0:T(8,128)(2,1)}, u32[]{:S(2)}, u32[]{:S(2)}) collective-permute-start(bf16[6144,128]{1,0:T(8,128)(2,1)} %pack.1.refs_0_), channel_id=1, source_target_pairs={{0,3},{16,28},{1,0},{17,29},{2,1},{18,30},{3,2},{19,31},{4,7},{20,... | collective-permute-start | bytes 4718600 | tf_op jit(solution)/shard_map/ppermute | solution.py:437
  57.3 27.5 %all-to-all-start.2 = ((bf16[4,4,384,128]{3,2,1,0:T(8,128)(2,1)}), bf16[4,4,384,128]{3,2,1,0:T(8,128)(2,1)S(1)}, u32[]{:S(2)}, u32[]{:S(2)}) async-start(bf16[4,4,384,128]{3,2,1,0:T(8,128)(2,1)} %broadcast_in_dim.21), calls=%async_computation.2 | async-start | bytes 3145728 | tf_op jit(solution)/shard_map/all_to_all | solution.py:20
  62.3 22.5 %collective-permute-start.2 = (bf16[3072,128]{1,0:T(8,128)(2,1)S(1)}, bf16[3072,128]{1,0:T(8,128)(2,1)}, u32[]{:S(2)}, u32[]{:S(2)}) collective-permute-start(bf16[3072,128]{1,0:T(8,128)(2,1)S(1)} %slice.260), channel_id=1, source_target_pairs={{0,1},{16,20},{1,2},{17,21},{2,3},{18,22},{3,0},{19,23},{4,5},{20,... | collective-permute-start | bytes 2359304 | tf_op jit(solution)/shard_map/ppermute | solution.py:455
  65.8 19.1 %collective-permute-start.3 = (bf16[3072,128]{1,0:T(8,128)(2,1)S(1)}, bf16[3072,128]{1,0:T(8,128)(2,1)}, u32[]{:S(2)}, u32[]{:S(2)}) collective-permute-start(bf16[3072,128]{1,0:T(8,128)(2,1)S(1)} %slice.261), channel_id=1, source_target_pairs={{0,3},{16,28},{1,0},{17,29},{2,1},{18,30},{3,2},{19,31},{4,7},{20,... | collective-permute-start | bytes 2359304 | tf_op jit(solution)/shard_map/ppermute | solution.py:456
  84.8 1.2 copy-start.2
  92.0 11.0 %all-to-all-start.3 = ((bf16[4,4,144,128]{3,2,1,0:T(8,128)(2,1)}), bf16[4,4,144,128]{3,2,1,0:T(8,128)(2,1)S(1)}, u32[]{:S(2)}, u32[]{:S(2)}) async-start(bf16[4,4,144,128]{3,2,1,0:T(8,128)(2,1)} %get-tuple-element.43), calls=%async_computation.3 | async-start | bytes 1179648 | tf_op jit(solution)/shard_map/all_to_all | solution.py:20
  98.9 28.3 %copy-start.9 = (f32[1024]{0:T(1024)S(1)}, f32[1024]{0:T(1024)}, u32[]{:S(2)}) copy-start(f32[1024]{0:T(1024)} %param.25) | copy-start | bytes 12292
  111.4 62.1 %collective-permute-start.4 = (bf16[5040,128]{1,0:T(8,128)(2,1)}, bf16[5040,128]{1,0:T(8,128)(2,1)S(1)}, u32[]{:S(2)}, u32[]{:S(2)}) collective-permute-start(bf16[5040,128]{1,0:T(8,128)(2,1)} %get-tuple-element.53.own_ref), channel_id=1, source_target_pairs={{0,1},{16,20},{1,2},{17,21},{2,3},{18,22},{3,0},{19,23},{4,5},{20,... | collective-permute-start | bytes 3870728 | tf_op jit(solution)/shard_map/ppermute | solution.py:526
  113.6 61.9 %collective-permute-start.5 = (bf16[5040,128]{1,0:T(8,128)(2,1)}, bf16[5040,128]{1,0:T(8,128)(2,1)S(1)}, u32[]{:S(2)}, u32[]{:S(2)}) collective-permute-start(bf16[5040,128]{1,0:T(8,128)(2,1)} %get-tuple-element.54), channel_id=1, source_target_pairs={{0,3},{16,28},{1,0},{17,29},{2,1},{18,30},{3,2},{19,31},{4,7},{20,... | collective-permute-start | bytes 3870728 | tf_op jit(solution)/shard_map/ppermute | solution.py:527
  117.9 28.0 %all-to-all-start.5 = ((bf16[32,24,128]{2,1,0:T(8,128)(2,1)}), bf16[32,24,128]{2,1,0:T(8,128)(2,1)S(1)}, u32[]{:S(2)}, u32[]{:S(2)}) async-start(bf16[32,24,128]{2,1,0:T(8,128)(2,1)} %bitcast.12), calls=%async_computation.5 | async-start | bytes 393216 | tf_op jit(solution)/shard_map/all_to_all | solution.py:20
  145.9 0.7 copy-start.5
  146.6 10.0 %copy-start.8 = (f32[64,31]{0,1:T(8,128)S(1)}, f32[64,31]{0,1:T(8,128)}, u32[]{:S(2)}) copy-start(f32[64,31]{0,1:T(8,128)} %param.23) | copy-start | bytes 23812
  146.6 23.8 %copy-start.1 = (f32[2,192]{1,0:T(2,128)S(1)}, f32[2,192]{1,0:T(2,128)}, u32[]{:S(2)}) copy-start(f32[2,192]{1,0:T(2,128)} %get-tuple-element.69.refs_3_) | copy-start | bytes 4612
  149.7 7.6 %collective-permute-start.9 = (bf16[16,32,128]{2,1,0:T(8,128)(2,1)}, bf16[16,32,128]{2,1,0:T(8,128)(2,1)S(1)}, u32[]{:S(2)}, u32[]{:S(2)}) collective-permute-start(bf16[16,32,128]{2,1,0:T(8,128)(2,1)} %get-tuple-element.65), channel_id=1, source_target_pairs={{0,16},{16,0},{1,17},{17,1},{2,18},{18,2},{3,19},{19,3},{4,20},{20... | collective-permute-start | bytes 393224 | tf_op jit(solution)/shard_map/ppermute | solution.py:577
  153.0 13.8 %all-to-all-start.6 = ((bf16[16,104,128]{2,1,0:T(8,128)(2,1)}), bf16[16,104,128]{2,1,0:T(8,128)(2,1)S(1)}, u32[]{:S(2)}, u32[]{:S(2)}) async-start(bf16[16,104,128]{2,1,0:T(8,128)(2,1)} %get-tuple-element.66), calls=%async_computation.6 | async-start | bytes 851968 | tf_op jit(solution)/shard_map/all_to_all | solution.py:20
  158.9 24.3 %copy-start.6 = (bf16[64,192]{1,0:T(8,128)(2,1)S(1)}, bf16[64,192]{1,0:T(8,128)(2,1)}, u32[]{:S(2)}) copy-start(bf16[64,192]{1,0:T(8,128)(2,1)} %param.22) | copy-start | bytes 73732
  166.8 19.6 %all-to-all-start.7 = ((bf16[16,32,128]{2,1,0:T(8,128)(2,1)}), bf16[16,32,128]{2,1,0:T(8,128)(2,1)S(1)}, u32[]{:S(2)}, u32[]{:S(2)}) async-start(bf16[16,32,128]{2,1,0:T(8,128)(2,1)} %add_convert_fusion), calls=%async_computation.7 | async-start | bytes 262144 | tf_op jit(solution)/shard_map/all_to_all | solution.py:20
  170.5 12.7 %collective-permute-start.10 = (f32[64,30]{1,0:T(8,128)S(1)}, f32[64,30]{1,0:T(8,128)S(1)}, u32[]{:S(2)}, u32[]{:S(2)}) collective-permute-start(f32[64,30]{1,0:T(8,128)S(1)} %get-tuple-element.71), channel_id=1, source_target_pairs={{16,0},{32,16},{48,32},{64,48},{80,64},{96,80},{112,96},{128,112},... | collective-permute-start | bytes 23048 | tf_op jit(solution)/shard_map/ppermute | solution.py:596
  173.6 15.8 %copy-start.3 = (bf16[5040,128]{1,0:T(8,128)(2,1)}, bf16[5040,128]{1,0:T(8,128)(2,1)S(1)}, u32[]{:S(2)}) copy-start(bf16[5040,128]{1,0:T(8,128)(2,1)S(1)} %collective-permute-done.4.behind_ref) | copy-start | bytes 3870724
  173.6 15.0 %collective-permute-start.6 = (bf16[2304,128]{1,0:T(8,128)(2,1)S(1)}, bf16[2304,128]{1,0:T(8,128)(2,1)}, u32[]{:S(2)}, u32[]{:S(2)}) collective-permute-start(bf16[2304,128]{1,0:T(8,128)(2,1)S(1)} %slice.262), channel_id=1, source_target_pairs={{0,1},{16,20},{1,2},{17,21},{2,3},{18,22},{3,0},{19,23},{4,5},{20,... | collective-permute-start | bytes 1769480 | tf_op jit(solution)/shard_map/ppermute | solution.py:530
  175.6 13.8 %copy-start.4 = (bf16[5040,128]{1,0:T(8,128)(2,1)}, bf16[5040,128]{1,0:T(8,128)(2,1)S(1)}, u32[]{:S(2)}) copy-start(bf16[5040,128]{1,0:T(8,128)(2,1)S(1)} %collective-permute-done.5.ahead_ref) | copy-start | bytes 3870724
  176.5 12.9 %collective-permute-start.7 = (bf16[2304,128]{1,0:T(8,128)(2,1)}, bf16[2304,128]{1,0:T(8,128)(2,1)}, u32[]{:S(2)}, u32[]{:S(2)}) collective-permute-start(bf16[2304,128]{1,0:T(8,128)(2,1)} %slice.263), channel_id=1, source_target_pairs={{0,3},{16,28},{1,0},{17,29},{2,1},{18,30},{3,2},{19,31},{4,7},{20,... | collective-permute-start | bytes 1769480 | tf_op jit(solution)/shard_map/ppermute | solution.py:531
  181.1 7.5 %collective-permute-start.8 = (bf16[432,128]{1,0:T(8,128)(2,1)}, bf16[432,128]{1,0:T(8,128)(2,1)S(1)}, u32[]{:S(2)}, u32[]{:S(2)}) collective-permute-start(bf16[432,128]{1,0:T(8,128)(2,1)} %get-tuple-element.55), channel_id=1, source_target_pairs={{0,2},{16,24},{1,3},{17,25},{2,0},{18,26},{3,1},{19,27},{4,6},{20,... | collective-permute-start | bytes 331784 | tf_op jit(solution)/shard_map/ppermute | solution.py:528
  188.6 0.8 copy-start.7

commit v2 on v1

--- a/solution.py
+++ b/solution.py
@@ -311,9 +311,12 @@
         copy.wait()
     moe = contract(back_ref[...], returned_ref[...], 0, 0)
     mix = (own_ref[...].astype(f32) + moe).astype(bf16)
-    for copy in copies[3:]:
-        copy.wait()
+    copies[3].wait()
     d_act = contract(proj_ref[...], mix, 1, 1)
+    copies[6].wait()
+    grad = jnp.dot(act_ref[...], mix, preferred_element_type=f32)
+    copies[4].wait()
+    copies[5].wait()
     lanes = 128
 
     def as_rows(line):
@@ -333,7 +336,6 @@
         blocks_ref[j, pl.ds(0, part), :] = wide.astype(bf16)
         blocks_ref[j, pl.ds(part, part // 2), :] = rest.astype(bf16)
         blocks_ref[j, pl.ds(part * 3 // 2, 8), :] = tail
-    grad = jnp.dot(act_ref[...], mix, preferred_element_type=f32)
     size = kept_ref.shape[1]
     for k in range(kept_ref.shape[0]):
         even = grad[2 * k * size : (2 * k + 1) * size]

time: 197 us -> 197 us (level)
  no operation moved by 1% of the time
where the time goes in v2:
time: 197 us; the launch traced here: 195 us
  starting transfers between devices  74.9 us (38%)
  waiting for transfers between devices  59.4 us (30%)
  Pallas kernels  28.3 us (14%)
  blocking collectives  17.8 us (9%)
  local copies, waits for them, and re-layouts  8.59 us (4%)
  other arithmetic  5.47 us (3%)
    all_to_all x6, waiting for transfers between devices, exchanged(): lax.all_to_all(blocks, axis, 0, 0, axis_index_groups=index_groups, tiled=...  42.3 us
    all_to_all x6, starting transfers between devices, exchanged(): lax.all_to_all(blocks, axis, 0, 0, axis_index_groups=index_groups, tiled=...  40.3 us
    all_to_all x2, blocking collectives, exchanged(): lax.all_to_all(blocks, axis, 0, 0, axis_index_groups=index_groups, tiled=...  17.8 us
    ppermute x1, waiting for transfers between devices, body(): lax.ppermute(weights[1][:middle], PLANE, onward)  14.8 us
    pallas_call x1, Pallas kernels, body(): pl.pallas_call(expert_kernel, in_specs=[scalar()] + [hbm] * 6, out_specs=...  5.96 us
    pallas_call x1, Pallas kernels, body(): pl.pallas_call(weight_kernel, in_specs=[whole()] * 8, out_specs=[whole()]...  5.51 us
    ppermute x1, starting transfers between devices, body(): far_high = lax.ppermute(from_ahead[far_rows:2 * far_rows], PLANE, backward)  4.56 us
    ppermute x1, starting transfers between devices, body(): from_ahead = lax.ppermute(to_backward, PLANE, backward)  4.3 us
  transfers between devices with their start and end apart: 17, of which 7 were waited for; matrix products, arithmetic and copies ran while one was open for 6% of the time, Pallas kernels for 7%

profile of v2, /device:TPU:1, one launch (start us, length us, event | category | flops | bytes accessed | tf_op | source)
XLA Modules:
  0.0 195.4 jit_solution(16864041545099761369)
XLA Ops:
  0.6 2.6 %prep.1 = (bf16[1280,128]{1,0:T(8,128)(2,1)}, bf16[768,192]{1,0:T(8,128)(2,1)}, bf16[192,128]{1,0:T(8,128)(2,1)}) custom-call(s32[1]{0:T(128)} %bitcast.1.refs_0_, s32[2,192]{1,0:T(2,128)} %bitcast.83, f32[2,192]{1,0:T(2,128)} %bitcast.84, bf16[192,2048]{1,0:T(8,128)(2,1)} %refs_3_.2, bf16[192,2048]{1,0:T(8,128)(2,1)} %refs_4_.1), custom_call_target="tpu_custom_call" | custom-call | tf_op jit(solution)/shard_map/prep/pallas_call | solution.py:399
  3.2 16.7 %all-to-all-start = ((bf16[32,40,128]{2,1,0:T(8,128)(2,1)}), bf16[32,40,128]{2,1,0:T(8,128)(2,1)S(1)}, u32[]{:S(2)}, u32[]{:S(2)}) async-start(bf16[32,40,128]{2,1,0:T(8,128)(2,1)} %bitcast.81), calls=%async_computation | async-start | bytes 655360 | tf_op jit(solution)/shard_map/all_to_all | solution.py:20
  20.0 2.7 %pack.1.refs_0_ = bf16[6144,128]{1,0:T(8,128)(2,1)} custom-call(bf16[2048,128]{1,0:T(8,128)(2,1)} %bitcast.85, bf16[2048,128]{1,0:T(8,128)(2,1)} %bitcast.86, bf16[128,2048]{1,0:T(8,128)(2,1)} %bitcast.87), custom_call_target="tpu_custom_call" | custom-call | flops 1207959552 | bytes 1572864 | tf_op jit(solution)/shard_map/pack/pallas_call | solution.py:426
  22.6 3.2 %collective-permute-start = (bf16[6144,128]{1,0:T(8,128)(2,1)}, bf16[6144,128]{1,0:T(8,128)(2,1)}, u32[]{:S(2)}, u32[]{:S(2)}) collective-permute-start(bf16[6144,128]{1,0:T(8,128)(2,1)} %pack.1.refs_0_), channel_id=1, source_target_pairs={{0,1},{16,20},{1,2},{17,21},{2,3},{18,22},{3,0},{19,23},{4,5},{20,... | collective-permute-start | bytes 4718600 | tf_op jit(solution)/shard_map/ppermute | solution.py:438
  25.8 3.4 %collective-permute-start.1 = (bf16[6144,128]{1,0:T(8,128)(2,1)}, bf16[6144,128]{1,0:T(8,128)(2,1)}, u32[]{:S(2)}, u32[]{:S(2)}) collective-permute-start(bf16[6144,128]{1,0:T(8,128)(2,1)} %pack.1.refs_0_), channel_id=1, source_target_pairs={{0,3},{16,28},{1,0},{17,29},{2,1},{18,30},{3,2},{19,31},{4,7},{20,... | collective-permute-start | bytes 4718600 | tf_op jit(solution)/shard_map/ppermute | solution.py:439
  29.2 15.7 %all-to-all-done = bf16[32,40,128]{2,1,0:T(8,128)(2,1)S(1)} async-done(((bf16[32,40,128]{2,1,0:T(8,128)(2,1)}), bf16[32,40,128]{2,1,0:T(8,128)(2,1)S(1)}, u32[]{:S(2)}, u32[]{:S(2)}) %all-to-all-start) | async-done | bytes 327712 | tf_op jit(solution)/shard_map/all_to_all | solution.py:20
  44.9 0.5 compact.1
  45.4 10.4 %all_to_all.40 = bf16[4,384,128]{2,1,0:T(8,128)(2,1)S(1)} all-to-all(bf16[4,384,128]{2,1,0:T(8,128)(2,1)S(1)} %compact.1), channel_id=1, replica_groups={{0,1,2,3},{4,5,6,7},{8,9,10,11},{12,13,14,15},{16,20,24,28},{17,21,25,2..., dimensions={0} | all-to-all | bytes 786432 | tf_op jit(solution)/shard_map/all_to_all | solution.py:20
  55.8 1.5 broadcast_in_dim.21
  57.3 3.8 %all-to-all-start.2 = ((bf16[4,4,384,128]{3,2,1,0:T(8,128)(2,1)}), bf16[4,4,384,128]{3,2,1,0:T(8,128)(2,1)S(1)}, u32[]{:S(2)}, u32[]{:S(2)}) async-start(bf16[4,4,384,128]{3,2,1,0:T(8,128)(2,1)} %broadcast_in_dim.21), calls=%async_computation.2 | async-start | bytes 3145728 | tf_op jit(solution)/shard_map/all_to_all | solution.py:20
  61.1 1.2 slice.260
  62.3 2.2 %collective-permute-start.2 = (bf16[3072,128]{1,0:T(8,128)(2,1)S(1)}, bf16[3072,128]{1,0:T(8,128)(2,1)}, u32[]{:S(2)}, u32[]{:S(2)}) collective-permute-start(bf16[3072,128]{1,0:T(8,128)(2,1)S(1)} %slice.260), channel_id=1, source_target_pairs={{0,1},{16,20},{1,2},{17,21},{2,3},{18,22},{3,0},{19,23},{4,5},{20,... | collective-permute-start | bytes 2359304 | tf_op jit(solution)/shard_map/ppermute | solution.py:457
  64.6 1.2 slice.261
  65.8 4.3 %collective-permute-start.3 = (bf16[3072,128]{1,0:T(8,128)(2,1)S(1)}, bf16[3072,128]{1,0:T(8,128)(2,1)}, u32[]{:S(2)}, u32[]{:S(2)}) collective-permute-start(bf16[3072,128]{1,0:T(8,128)(2,1)S(1)} %slice.261), channel_id=1, source_target_pairs={{0,3},{16,28},{1,0},{17,29},{2,1},{18,30},{3,2},{19,31},{4,7},{20,... | collective-permute-start | bytes 2359304 | tf_op jit(solution)/shard_map/ppermute | solution.py:458
  70.0 14.8 %collective-permute-done.2.refs_3_ = bf16[3072,128]{1,0:T(8,128)(2,1)} collective-permute-done((bf16[3072,128]{1,0:T(8,128)(2,1)S(1)}, bf16[3072,128]{1,0:T(8,128)(2,1)}, u32[]{:S(2)}, u32[]{:S(2)}) %collective-permute-start.2) | collective-permute-done | bytes 786464 | tf_op jit(solution)/shard_map/ppermute | solution.py:457
  84.8 1.2 copy-done.2
  86.0 6.0 %expert.1 = (bf16[4,4,144,128]{3,2,1,0:T(8,128)(2,1)}, bf16[144,512]{1,0:T(8,128)(2,1)}, bf16[144,1024]{1,0:T(8,128)(2,1)}) custom-call(s32[1]{0:T(128)} %bitcast.core_ref, bf16[4,4,384,128]{3,2,1,0:T(8,128)(2,1)} %copy-done.2, bf16[6144,128]{1,0:T(8,128)(2,1)} %pack.1.refs_0_, bf16[6144,128]{1,0:T(8,128)(2,1)} %collective-permute-done.refs_1_, ...), custom_call_target="tpu_custom_call" | custom-call | flops 1509949440 | bytes 11796480 | tf_op jit(solution)/shard_map/expert/pallas_call | solution.py:463
  92.0 3.5 %all-to-all-start.3 = ((bf16[4,4,144,128]{3,2,1,0:T(8,128)(2,1)}), bf16[4,4,144,128]{3,2,1,0:T(8,128)(2,1)S(1)}, u32[]{:S(2)}, u32[]{:S(2)}) async-start(bf16[4,4,144,128]{3,2,1,0:T(8,128)(2,1)} %get-tuple-element.43), calls=%async_computation.3 | async-start | bytes 1179648 | tf_op jit(solution)/shard_map/all_to_all | solution.py:20
  95.5 3.4 %row_pack.1 = (bf16[5040,128]{1,0:T(8,128)(2,1)}, bf16[5040,128]{1,0:T(8,128)(2,1)}, bf16[432,128]{1,0:T(8,128)(2,1)}) custom-call(s32[1]{0:T(128)} %bitcast.core_ref, bf16[4,4,384,128]{3,2,1,0:T(8,128)(2,1)} %copy-done.2, bf16[144,512]{1,0:T(8,128)(2,1)} %get-tuple-element.44.hidden_ref, bf16[144,1024]{1,0:T(8,128)(2,1)} %get-tuple-element.45.both_ref), custom_call_target="tpu_custom_call" | custom-call | flops 905969664 | bytes 11796480 | tf_op jit(solution)/shard_map/row_pack/pallas_call | solution.py:489
  98.9 4.1 %all-to-all-done.3.parts_ref = bf16[4,4,144,128]{3,2,1,0:T(8,128)(2,1)S(1)} async-done(((bf16[4,4,144,128]{3,2,1,0:T(8,128)(2,1)}), bf16[4,4,144,128]{3,2,1,0:T(8,128)(2,1)S(1)}, u32[]{:S(2)}, u32[]{:S(2)}) %all-to-all-start.3) | async-done | bytes 589856 | tf_op jit(solution)/shard_map/all_to_all | solution.py:20
  103.1 7.4 %all_to_all.41.refs_0_ = bf16[4,144,128]{2,1,0:T(8,128)(2,1)S(1)} all-to-all(bf16[4,144,128]{2,1,0:T(8,128)(2,1)S(1)} %line_sum.1), channel_id=1, replica_groups={{0,1,2,3},{4,5,6,7},{8,9,10,11},{12,13,14,15},{16,20,24,28},{17,21,25,2..., dimensions={0} | all-to-all | bytes 294912 | tf_op jit(solution)/shard_map/all_to_all | solution.py:20
  110.5 0.9 spread.1
  111.4 2.2 %collective-permute-start.4 = (bf16[5040,128]{1,0:T(8,128)(2,1)}, bf16[5040,128]{1,0:T(8,128)(2,1)S(1)}, u32[]{:S(2)}, u32[]{:S(2)}) collective-permute-start(bf16[5040,128]{1,0:T(8,128)(2,1)} %get-tuple-element.53.own_ref), channel_id=1, source_target_pairs={{0,1},{16,20},{1,2},{17,21},{2,3},{18,22},{3,0},{19,23},{4,5},{20,... | collective-permute-start | bytes 3870728 | tf_op jit(solution)/shard_map/ppermute | solution.py:528
  113.6 4.3 %collective-permute-start.5 = (bf16[5040,128]{1,0:T(8,128)(2,1)}, bf16[5040,128]{1,0:T(8,128)(2,1)S(1)}, u32[]{:S(2)}, u32[]{:S(2)}) collective-permute-start(bf16[5040,128]{1,0:T(8,128)(2,1)} %get-tuple-element.54), channel_id=1, source_target_pairs={{0,3},{16,28},{1,0},{17,29},{2,1},{18,30},{3,2},{19,31},{4,7},{20,... | collective-permute-start | bytes 3870728 | tf_op jit(solution)/shard_map/ppermute | solution.py:529
  117.9 9.2 %all-to-all-start.5 = ((bf16[32,24,128]{2,1,0:T(8,128)(2,1)}), bf16[32,24,128]{2,1,0:T(8,128)(2,1)S(1)}, u32[]{:S(2)}, u32[]{:S(2)}) async-start(bf16[32,24,128]{2,1,0:T(8,128)(2,1)} %bitcast.12), calls=%async_computation.5 | async-start | bytes 393216 | tf_op jit(solution)/shard_map/all_to_all | solution.py:20
  127.1 1.0 copy.20.gain_ref
  128.3 3.1 %norm.1 = (bf16[1024,192]{1,0:T(8,128)(2,1)}, bf16[1024,192]{1,0:T(8,128)(2,1)}, bf16[1024,192]{1,0:T(8,128)(2,1)}, f32[2,192]{1,0:T(2,128)}) custom-call(s32[1]{0:T(128)} %bitcast.core_ref, bf16[4,4,384,128]{3,2,1,0:T(8,128)(2,1)} %copy-done.2, f32[1024,1]{1,0:T(8,128)} %copy.20.gain_ref), custom_call_target="tpu_custom_call" | custom-call | flops 905969664 | bytes 11796480 | tf_op jit(solution)/shard_map/norm/pallas_call | solution.py:535
  131.5 14.5 %all-to-all-done.5 = bf16[32,24,128]{2,1,0:T(8,128)(2,1)S(1)} async-done(((bf16[32,24,128]{2,1,0:T(8,128)(2,1)}), bf16[32,24,128]{2,1,0:T(8,128)(2,1)S(1)}, u32[]{:S(2)}, u32[]{:S(2)}) %all-to-all-start.5) | async-done | bytes 196640 | tf_op jit(solution)/shard_map/all_to_all | solution.py:20
  145.9 0.7 copy-done.5
  146.6 3.5 %mix.1 = (bf16[16,32,128]{2,1,0:T(8,128)(2,1)}, bf16[16,32,128]{2,1,0:T(8,128)(2,1)}, bf16[16,104,128]{2,1,0:T(8,128)(2,1)}) custom-call(s32[1]{0:T(128)} %bitcast.core_ref, bf16[768,192]{1,0:T(8,128)(2,1)} %get-tuple-element.59.refs_0_, bf16[768,128]{1,0:T(8,128)(2,1)} %bitcast.80, bf16[192,128]{1,0:T(8,128)(2,1)} %get-tuple-element.60.refs_2_, ...), custom_call_target="tpu_custom_call" | custom-call | tf_op jit(solution)/shard_map/mix/pallas_call | solution.py:564
  150.1 3.4 %collective-permute-start.9 = (bf16[16,32,128]{2,1,0:T(8,128)(2,1)}, bf16[16,32,128]{2,1,0:T(8,128)(2,1)S(1)}, u32[]{:S(2)}, u32[]{:S(2)}) collective-permute-start(bf16[16,32,128]{2,1,0:T(8,128)(2,1)} %get-tuple-element.65), channel_id=1, source_target_pairs={{0,16},{16,0},{1,17},{17,1},{2,18},{18,2},{3,19},{19,3},{4,20},{20... | collective-permute-start | bytes 393224 | tf_op jit(solution)/shard_map/ppermute | solution.py:579
  153.5 3.6 %all-to-all-start.6 = ((bf16[16,104,128]{2,1,0:T(8,128)(2,1)}), bf16[16,104,128]{2,1,0:T(8,128)(2,1)S(1)}, u32[]{:S(2)}, u32[]{:S(2)}) async-start(bf16[16,104,128]{2,1,0:T(8,128)(2,1)} %get-tuple-element.66), calls=%async_computation.6 | async-start | bytes 851968 | tf_op jit(solution)/shard_map/all_to_all | solution.py:20
  157.1 0.7 slice_bitcast_fusion.30
  157.8 1.6 add_convert_fusion
  159.4 7.9 %all-to-all-done.6.refs_0_ = bf16[16,104,128]{2,1,0:T(8,128)(2,1)S(1)} async-done(((bf16[16,104,128]{2,1,0:T(8,128)(2,1)}), bf16[16,104,128]{2,1,0:T(8,128)(2,1)S(1)}, u32[]{:S(2)}, u32[]{:S(2)}) %all-to-all-start.6) | async-done | bytes 426016 | tf_op jit(solution)/shard_map/all_to_all | solution.py:20
  167.3 3.5 %all-to-all-start.7 = ((bf16[16,32,128]{2,1,0:T(8,128)(2,1)}), bf16[16,32,128]{2,1,0:T(8,128)(2,1)S(1)}, u32[]{:S(2)}, u32[]{:S(2)}) async-start(bf16[16,32,128]{2,1,0:T(8,128)(2,1)} %add_convert_fusion), calls=%async_computation.7 | async-start | bytes 262144 | tf_op jit(solution)/shard_map/all_to_all | solution.py:20
  170.9 0.1 conv_grad.1
  171.0 3.1 %collective-permute-start.10 = (f32[64,30]{1,0:T(8,128)S(1)}, f32[64,30]{1,0:T(8,128)S(1)}, u32[]{:S(2)}, u32[]{:S(2)}) collective-permute-start(f32[64,30]{1,0:T(8,128)S(1)} %get-tuple-element.71), channel_id=1, source_target_pairs={{16,0},{32,16},{48,32},{64,48},{80,64},{96,80},{112,96},{128,112},... | collective-permute-start | bytes 23048 | tf_op jit(solution)/shard_map/ppermute | solution.py:598
  174.1 1.9 collective-permute-start.6
  176.1 0.9 slice.263
  177.0 4.6 %collective-permute-start.7 = (bf16[2304,128]{1,0:T(8,128)(2,1)}, bf16[2304,128]{1,0:T(8,128)(2,1)}, u32[]{:S(2)}, u32[]{:S(2)}) collective-permute-start(bf16[2304,128]{1,0:T(8,128)(2,1)} %slice.263), channel_id=1, source_target_pairs={{0,3},{16,28},{1,0},{17,29},{2,1},{18,30},{3,2},{19,31},{4,7},{20,... | collective-permute-start | bytes 1769480 | tf_op jit(solution)/shard_map/ppermute | solution.py:533
  181.6 2.1 %collective-permute-start.8 = (bf16[432,128]{1,0:T(8,128)(2,1)}, bf16[432,128]{1,0:T(8,128)(2,1)S(1)}, u32[]{:S(2)}, u32[]{:S(2)}) collective-permute-start(bf16[432,128]{1,0:T(8,128)(2,1)} %get-tuple-element.55), channel_id=1, source_target_pairs={{0,2},{16,24},{1,3},{17,25},{2,0},{18,26},{3,1},{19,27},{4,6},{20,... | collective-permute-start | bytes 331784 | tf_op jit(solution)/shard_map/ppermute | solution.py:530
  183.7 2.6 %multiply_convert_fusion = (bf16[64,192]{1,0:T(8,128)(2,1)}, f32[64,192]{1,0:T(8,128)S(1)}) fusion(bf16[64,192]{1,0:T(8,128)(2,1)} %param.21, bf16[64,192]{1,0:T(8,128)(2,1)S(1)} %copy-done.6, f32[64,192]{1,0:T(8,128)S(1)} %get-tuple-element.70, f32[64]{0:T(128)S(1)} %get-tuple-element.103, f32[64,30]{1,0:T(8,128)S(1)} %collective-permute-done.10, ...), kind=kLoop, calls=%fused_computation.129 | loop fusion | flops 1241088 | bytes 187648 | tf_op jit(solution)/shard_map/convert_element_type | solution.py:611
  186.3 0.6 multiply_convert_fusion.1
  186.9 0.6 convert_reduce_fusion
  187.6 1.5 collective-permute-done.8.across_ref
  189.1 0.8 collective-permute-done.7.high_ref
  189.9 5.5 %weight_sum.1 = (bf16[2048,128]{1,0:T(8,128)(2,1)}, bf16[2048,128]{1,0:T(8,128)(2,1)}, bf16[128,2048]{1,0:T(8,128)(2,1)}) custom-call(bf16[5040,128]{1,0:T(8,128)(2,1)} %get-tuple-element.53.own_ref, bf16[5040,128]{1,0:T(8,128)(2,1)} %copy-done.3, bf16[5040,128]{1,0:T(8,128)(2,1)} %copy-done.4, bf16[2304,128]{1,0:T(8,128)(2,1)} %collective-permute-done.6.low_ref, ...), custom_call_target="tpu_custom_call" | custom-call | flops 905969664 | bytes 11796480 | tf_op jit(solution)/shard_map/weight_sum/pallas_call | solution.py:612
  (33 shorter events, 0.4 us)
Async XLA Ops:
  3.2 41.7 %all-to-all-start = ((bf16[32,40,128]{2,1,0:T(8,128)(2,1)}), bf16[32,40,128]{2,1,0:T(8,128)(2,1)S(1)}, u32[]{:S(2)}, u32[]{:S(2)}) async-start(bf16[32,40,128]{2,1,0:T(8,128)(2,1)} %bitcast.81), calls=%async_computation | async-start | bytes 655360 | tf_op jit(solution)/shard_map/all_to_all | solution.py:20
  20.0 25.0 %copy-start = (bf16[64,192]{1,0:T(8,128)(2,1)S(1)}, bf16[64,192]{1,0:T(8,128)(2,1)}, u32[]{:S(2)}) copy-start(bf16[64,192]{1,0:T(8,128)(2,1)} %refs_1_.3) | copy-start | bytes 73732
  22.6 38.5 %collective-permute-start = (bf16[6144,128]{1,0:T(8,128)(2,1)}, bf16[6144,128]{1,0:T(8,128)(2,1)}, u32[]{:S(2)}, u32[]{:S(2)}) collective-permute-start(bf16[6144,128]{1,0:T(8,128)(2,1)} %pack.1.refs_0_), channel_id=1, source_target_pairs={{0,1},{16,20},{1,2},{17,21},{2,3},{18,22},{3,0},{19,23},{4,5},{20,... | collective-permute-start | bytes 4718600 | tf_op jit(solution)/shard_map/ppermute | solution.py:438
  25.8 38.7 %collective-permute-start.1 = (bf16[6144,128]{1,0:T(8,128)(2,1)}, bf16[6144,128]{1,0:T(8,128)(2,1)}, u32[]{:S(2)}, u32[]{:S(2)}) collective-permute-start(bf16[6144,128]{1,0:T(8,128)(2,1)} %pack.1.refs_0_), channel_id=1, source_target_pairs={{0,3},{16,28},{1,0},{17,29},{2,1},{18,30},{3,2},{19,31},{4,7},{20,... | collective-permute-start | bytes 4718600 | tf_op jit(solution)/shard_map/ppermute | solution.py:439
  57.3 27.5 %all-to-all-start.2 = ((bf16[4,4,384,128]{3,2,1,0:T(8,128)(2,1)}), bf16[4,4,384,128]{3,2,1,0:T(8,128)(2,1)S(1)}, u32[]{:S(2)}, u32[]{:S(2)}) async-start(bf16[4,4,384,128]{3,2,1,0:T(8,128)(2,1)} %broadcast_in_dim.21), calls=%async_computation.2 | async-start | bytes 3145728 | tf_op jit(solution)/shard_map/all_to_all | solution.py:20
  62.3 22.5 %collective-permute-start.2 = (bf16[3072,128]{1,0:T(8,128)(2,1)S(1)}, bf16[3072,128]{1,0:T(8,128)(2,1)}, u32[]{:S(2)}, u32[]{:S(2)}) collective-permute-start(bf16[3072,128]{1,0:T(8,128)(2,1)S(1)} %slice.260), channel_id=1, source_target_pairs={{0,1},{16,20},{1,2},{17,21},{2,3},{18,22},{3,0},{19,23},{4,5},{20,... | collective-permute-start | bytes 2359304 | tf_op jit(solution)/shard_map/ppermute | solution.py:457
  65.8 19.1 %collective-permute-start.3 = (bf16[3072,128]{1,0:T(8,128)(2,1)S(1)}, bf16[3072,128]{1,0:T(8,128)(2,1)}, u32[]{:S(2)}, u32[]{:S(2)}) collective-permute-start(bf16[3072,128]{1,0:T(8,128)(2,1)S(1)} %slice.261), channel_id=1, source_target_pairs={{0,3},{16,28},{1,0},{17,29},{2,1},{18,30},{3,2},{19,31},{4,7},{20,... | collective-permute-start | bytes 2359304 | tf_op jit(solution)/shard_map/ppermute | solution.py:458
  84.8 1.2 copy-start.2
  92.0 11.0 %all-to-all-start.3 = ((bf16[4,4,144,128]{3,2,1,0:T(8,128)(2,1)}), bf16[4,4,144,128]{3,2,1,0:T(8,128)(2,1)S(1)}, u32[]{:S(2)}, u32[]{:S(2)}) async-start(bf16[4,4,144,128]{3,2,1,0:T(8,128)(2,1)} %get-tuple-element.43), calls=%async_computation.3 | async-start | bytes 1179648 | tf_op jit(solution)/shard_map/all_to_all | solution.py:20
  98.9 28.3 %copy-start.9 = (f32[1024]{0:T(1024)S(1)}, f32[1024]{0:T(1024)}, u32[]{:S(2)}) copy-start(f32[1024]{0:T(1024)} %param.25) | copy-start | bytes 12292
  111.4 62.6 %collective-permute-start.4 = (bf16[5040,128]{1,0:T(8,128)(2,1)}, bf16[5040,128]{1,0:T(8,128)(2,1)S(1)}, u32[]{:S(2)}, u32[]{:S(2)}) collective-permute-start(bf16[5040,128]{1,0:T(8,128)(2,1)} %get-tuple-element.53.own_ref), channel_id=1, source_target_pairs={{0,1},{16,20},{1,2},{17,21},{2,3},{18,22},{3,0},{19,23},{4,5},{20,... | collective-permute-start | bytes 3870728 | tf_op jit(solution)/shard_map/ppermute | solution.py:528
  113.6 62.4 %collective-permute-start.5 = (bf16[5040,128]{1,0:T(8,128)(2,1)}, bf16[5040,128]{1,0:T(8,128)(2,1)S(1)}, u32[]{:S(2)}, u32[]{:S(2)}) collective-permute-start(bf16[5040,128]{1,0:T(8,128)(2,1)} %get-tuple-element.54), channel_id=1, source_target_pairs={{0,3},{16,28},{1,0},{17,29},{2,1},{18,30},{3,2},{19,31},{4,7},{20,... | collective-permute-start | bytes 3870728 | tf_op jit(solution)/shard_map/ppermute | solution.py:529
  117.9 28.0 %all-to-all-start.5 = ((bf16[32,24,128]{2,1,0:T(8,128)(2,1)}), bf16[32,24,128]{2,1,0:T(8,128)(2,1)S(1)}, u32[]{:S(2)}, u32[]{:S(2)}) async-start(bf16[32,24,128]{2,1,0:T(8,128)(2,1)} %bitcast.12), calls=%async_computation.5 | async-start | bytes 393216 | tf_op jit(solution)/shard_map/all_to_all | solution.py:20
  145.9 0.7 copy-start.5
  146.6 10.5 %copy-start.8 = (f32[64,31]{0,1:T(8,128)S(1)}, f32[64,31]{0,1:T(8,128)}, u32[]{:S(2)}) copy-start(f32[64,31]{0,1:T(8,128)} %param.23) | copy-start | bytes 23812
  146.6 24.2 %copy-start.1 = (f32[2,192]{1,0:T(2,128)S(1)}, f32[2,192]{1,0:T(2,128)}, u32[]{:S(2)}) copy-start(f32[2,192]{1,0:T(2,128)} %get-tuple-element.69.refs_3_) | copy-start | bytes 4612
  150.1 7.6 %collective-permute-start.9 = (bf16[16,32,128]{2,1,0:T(8,128)(2,1)}, bf16[16,32,128]{2,1,0:T(8,128)(2,1)S(1)}, u32[]{:S(2)}, u32[]{:S(2)}) collective-permute-start(bf16[16,32,128]{2,1,0:T(8,128)(2,1)} %get-tuple-element.65), channel_id=1, source_target_pairs={{0,16},{16,0},{1,17},{17,1},{2,18},{18,2},{3,19},{19,3},{4,20},{20... | collective-permute-start | bytes 393224 | tf_op jit(solution)/shard_map/ppermute | solution.py:579
  153.5 13.8 %all-to-all-start.6 = ((bf16[16,104,128]{2,1,0:T(8,128)(2,1)}), bf16[16,104,128]{2,1,0:T(8,128)(2,1)S(1)}, u32[]{:S(2)}, u32[]{:S(2)}) async-start(bf16[16,104,128]{2,1,0:T(8,128)(2,1)} %get-tuple-element.66), calls=%async_computation.6 | async-start | bytes 851968 | tf_op jit(solution)/shard_map/all_to_all | solution.py:20
  159.4 24.3 %copy-start.6 = (bf16[64,192]{1,0:T(8,128)(2,1)S(1)}, bf16[64,192]{1,0:T(8,128)(2,1)}, u32[]{:S(2)}) copy-start(bf16[64,192]{1,0:T(8,128)(2,1)} %param.22) | copy-start | bytes 73732
  167.3 19.6 %all-to-all-start.7 = ((bf16[16,32,128]{2,1,0:T(8,128)(2,1)}), bf16[16,32,128]{2,1,0:T(8,128)(2,1)S(1)}, u32[]{:S(2)}, u32[]{:S(2)}) async-start(bf16[16,32,128]{2,1,0:T(8,128)(2,1)} %add_convert_fusion), calls=%async_computation.7 | async-start | bytes 262144 | tf_op jit(solution)/shard_map/all_to_all | solution.py:20
  171.0 12.7 %collective-permute-start.10 = (f32[64,30]{1,0:T(8,128)S(1)}, f32[64,30]{1,0:T(8,128)S(1)}, u32[]{:S(2)}, u32[]{:S(2)}) collective-permute-start(f32[64,30]{1,0:T(8,128)S(1)} %get-tuple-element.71), channel_id=1, source_target_pairs={{16,0},{32,16},{48,32},{64,48},{80,64},{96,80},{112,96},{128,112},... | collective-permute-start | bytes 23048 | tf_op jit(solution)/shard_map/ppermute | solution.py:598
  174.1 15.8 %copy-start.3 = (bf16[5040,128]{1,0:T(8,128)(2,1)}, bf16[5040,128]{1,0:T(8,128)(2,1)S(1)}, u32[]{:S(2)}) copy-start(bf16[5040,128]{1,0:T(8,128)(2,1)S(1)} %collective-permute-done.4.behind_ref) | copy-start | bytes 3870724
  174.1 15.0 %collective-permute-start.6 = (bf16[2304,128]{1,0:T(8,128)(2,1)S(1)}, bf16[2304,128]{1,0:T(8,128)(2,1)}, u32[]{:S(2)}, u32[]{:S(2)}) collective-permute-start(bf16[2304,128]{1,0:T(8,128)(2,1)S(1)} %slice.262), channel_id=1, source_target_pairs={{0,1},{16,20},{1,2},{17,21},{2,3},{18,22},{3,0},{19,23},{4,5},{20,... | collective-permute-start | bytes 1769480 | tf_op jit(solution)/shard_map/ppermute | solution.py:532
  176.1 13.8 %copy-start.4 = (bf16[5040,128]{1,0:T(8,128)(2,1)}, bf16[5040,128]{1,0:T(8,128)(2,1)S(1)}, u32[]{:S(2)}) copy-start(bf16[5040,128]{1,0:T(8,128)(2,1)S(1)} %collective-permute-done.5.ahead_ref) | copy-start | bytes 3870724
  177.0 12.9 %collective-permute-start.7 = (bf16[2304,128]{1,0:T(8,128)(2,1)}, bf16[2304,128]{1,0:T(8,128)(2,1)}, u32[]{:S(2)}, u32[]{:S(2)}) collective-permute-start(bf16[2304,128]{1,0:T(8,128)(2,1)} %slice.263), channel_id=1, source_target_pairs={{0,3},{16,28},{1,0},{17,29},{2,1},{18,30},{3,2},{19,31},{4,7},{20,... | collective-permute-start | bytes 1769480 | tf_op jit(solution)/shard_map/ppermute | solution.py:533
  181.6 7.5 %collective-permute-start.8 = (bf16[432,128]{1,0:T(8,128)(2,1)}, bf16[432,128]{1,0:T(8,128)(2,1)S(1)}, u32[]{:S(2)}, u32[]{:S(2)}) collective-permute-start(bf16[432,128]{1,0:T(8,128)(2,1)} %get-tuple-element.55), channel_id=1, source_target_pairs={{0,2},{16,24},{1,3},{17,25},{2,0},{18,26},{3,1},{19,27},{4,6},{20,... | collective-permute-start | bytes 331784 | tf_op jit(solution)/shard_map/ppermute | solution.py:530
  189.1 0.8 copy-start.7
